TPU v7x, 128 devices: a whole 4x4x4 slice. The times are simulated.
128 devices in a mesh: ep: 128 (over z, y, x, core).
Axes of the slice: x: 4, y: 4, z: 4, core: 2. Of those that a mesh axis runs over, the one named last changes fastest.
Arguments:
- tokens: bfloat16 [2048, 1024], P('ep'), may hold values from -6 to 6
- lengths: int32 [2048], P('ep'), may hold values from 1 to 8191
- cache_keys: bfloat16 [2048, 128, 512], P('ep'), may hold values from -6 to 6
- cache_values: bfloat16 [2048, 128, 1024], P('ep'), may hold values from -6 to 6
- retention_state: float32 [2048, 4, 128, 256], P('ep'), may hold values from -24 to 24
- mix_gain: float32 [1024], replicated, may hold values from 0.1 to 1.9
- query_weight: bfloat16 [1024, 512], replicated, may hold values from -0.1875 to 0.1875
- key_weight: bfloat16 [1024, 512], replicated, may hold values from -0.1875 to 0.1875
- value_weight: bfloat16 [1024, 1024], replicated, may hold values from -0.1875 to 0.1875
- out_weight: bfloat16 [1024, 1024], replicated, may hold values from -0.1875 to 0.1875
- ffn_gain: float32 [1024], replicated, may hold values from 0.1 to 1.9
- routes: int32 [2048, 6], P('ep'), may hold values from 0 to 127, all different within a row; in each aligned block of 16 rows (0 to 15, 16 to 31, ...) at most 2 rows name the same one
- route_scores: float32 [2048, 6], P('ep'), may hold values from 0.05 to 1
- expert_gate: bfloat16 [128, 1024, 256], P('ep'), may hold values from -0.1875 to 0.1875
- expert_up: bfloat16 [128, 1024, 256], P('ep'), may hold values from -0.1875 to 0.1875
- expert_down: bfloat16 [128, 256, 1024], P('ep'), may hold values from -0.375 to 0.375
- shared_gate: bfloat16 [1024, 256], replicated, may hold values from -0.1875 to 0.1875
- shared_up: bfloat16 [1024, 256], replicated, may hold values from -0.1875 to 0.1875
- shared_down: bfloat16 [256, 1024], replicated, may hold values from -0.375 to 0.375
- dense_gate: bfloat16 [4096, 1024], P('ep'), may hold values from -0.1875 to 0.1875
- dense_up: bfloat16 [4096, 1024], P('ep'), may hold values from -0.1875 to 0.1875
- dense_down: bfloat16 [4096, 1024], P('ep'), may hold values from -0.09375 to 0.09375
- dense_mix: float32 [1024], replicated, may hold values from -3 to 3
Outputs:
- layer_out: bfloat16 [2048, 1024], P('ep')
- new_keys: bfloat16 [2048, 512], P('ep')
- new_values: bfloat16 [2048, 1024], P('ep')
Inputs may be any that keep to these rules, and one draw needn't show every extreme that they name: `routes`: each row names 6 different experts; among the rows of one device no expert is named more than 2 times.
All inputs are finite; a program needn't handle non-finite values.
Results may differ from a plain program's by a relative error of at most 0.012.
Values may be sent and summed in bfloat16 or wider, within the bound.
A program may use at most 128 MiB of HBM per device.

v0:
```python
import jax
import jax.numpy as jnp
from jax import lax
from jax.sharding import PartitionSpec as P

eps = 1e-06
route_scale = 2.5
rope_base = 10000.0


def side_by_side(arrays, axis, dim, along):
    ends, at = ([], 0)
    for a in arrays[:-1]:
        at += a.shape[along]
        ends.append(at)
    both = jnp.concatenate(arrays, axis=along)
    return tuple(jnp.split(lax.all_gather(both, axis, axis=dim, tiled=True), ends, axis=along))


def normed(values):
    return values * lax.rsqrt(jnp.mean(values * values, axis=-1, keepdims=True) + eps)


def log_decay(head_count):
    return jnp.log1p(-jnp.exp2(-5.0 - jnp.arange(head_count, dtype=jnp.float32)))


def rotate(values, positions):
    half_size = values.shape[-1] // 2
    inverse = rope_base ** (-jnp.arange(half_size, dtype=jnp.float32) / half_size)
    angles = positions.astype(jnp.float32)[:, None, None] * inverse[None, None, :]
    cosine = jnp.cos(angles)
    sine_part = jnp.sin(angles)
    first_half = values[..., :half_size]
    second = values[..., half_size:]
    return jnp.concatenate(
        [first_half * cosine - second * sine_part, first_half * sine_part + second * cosine],
        axis=-1,
    )


def swiglu(inputs, w_gate, w_up, w_down):
    gate_part = jnp.dot(inputs, w_gate, preferred_element_type=jnp.float32)
    up_part = jnp.dot(inputs, w_up, preferred_element_type=jnp.float32)
    hidden = (jax.nn.silu(gate_part) * up_part).astype(jnp.bfloat16)
    return jnp.dot(hidden, w_down, preferred_element_type=jnp.float32)


def dense_part(inputs, gate_rows, up_rows, down_rows):
    contract = (((1,), (1,)), ((), ()))
    gate_part = lax.dot_general(inputs, gate_rows, contract, preferred_element_type=jnp.float32)
    up_part = lax.dot_general(inputs, up_rows, contract, preferred_element_type=jnp.float32)
    hidden = (jax.nn.silu(gate_part) * up_part).astype(jnp.bfloat16)
    return jnp.dot(hidden, down_rows, preferred_element_type=jnp.float32)


def retain(
    tokens, lengths, mix_gain, w_query, w_key, w_value, w_out, cache_keys, cache_values, carry_state
):
    seq_count, head_count, key_size, value_size = carry_state.shape
    block_size = cache_keys.shape[1]
    widened = tokens.astype(jnp.float32)
    normal_in = (normed(widened) * mix_gain).astype(jnp.bfloat16)
    raw_query = jnp.dot(normal_in, w_query, preferred_element_type=jnp.float32).reshape(
        seq_count, head_count, key_size
    )
    raw_key = jnp.dot(normal_in, w_key, preferred_element_type=jnp.float32).reshape(
        seq_count, head_count, key_size
    )
    raw_value = jnp.dot(normal_in, w_value, preferred_element_type=jnp.float32).reshape(
        seq_count, head_count, value_size
    )
    queries = (rotate(raw_query, lengths) * key_size ** (-0.5)).astype(jnp.bfloat16)
    new_keys = rotate(raw_key, lengths).astype(jnp.bfloat16)
    new_values = raw_value.astype(jnp.bfloat16)
    filled = lengths % block_size
    decay_rate = log_decay(head_count)
    places = jnp.arange(block_size, dtype=jnp.int32)
    stored_keys = cache_keys.reshape(seq_count, block_size, head_count, key_size)
    stored_values = cache_values.reshape(seq_count, block_size, head_count, value_size)
    scores = jnp.einsum("shd,sjhd->shj", queries, stored_keys, preferred_element_type=jnp.float32)
    distance = jnp.maximum(filled[:, None] - places[None, :], 0).astype(jnp.float32)
    live_mask = places[None, :] < filled[:, None]
    weighted = jnp.where(
        live_mask[:, None, :],
        scores * jnp.exp(distance[:, None, :] * decay_rate[None, :, None]),
        0.0,
    ).astype(jnp.bfloat16)
    own_weight = jnp.sum(
        queries.astype(jnp.float32) * new_keys.astype(jnp.float32), axis=-1
    ).astype(jnp.bfloat16)
    inside = jnp.einsum(
        "shj,sjhe->she", weighted, stored_values, preferred_element_type=jnp.float32
    )
    inside = inside + own_weight.astype(jnp.float32)[:, :, None] * new_values.astype(jnp.float32)
    carried = jnp.einsum("shd,shde->she", queries.astype(jnp.float32), carry_state)
    carried = (
        carried
        * jnp.exp((filled.astype(jnp.float32)[:, None] + 1.0) * decay_rate[None, :])[:, :, None]
    )
    headed = (
        normed(inside + carried).astype(jnp.bfloat16).reshape(seq_count, head_count * value_size)
    )
    mixer_out = jnp.dot(headed, w_out, preferred_element_type=jnp.float32)
    residual = widened + normed(mixer_out)
    return (
        residual,
        new_keys.reshape(seq_count, head_count * key_size),
        new_values.reshape(seq_count, head_count * value_size),
    )


def capacity(seq_count, top_count, expert_count):
    return max(2, seq_count * top_count * 8 // (3 * expert_count))


def exchanged_experts(normal_ffn, routes, route_weight, expert_gate, expert_up, expert_down):
    seq_count, top_count = routes.shape
    model_width = normal_ffn.shape[1]
    expert_count = lax.axis_size("ep") * expert_gate.shape[0]
    slot_count = capacity(seq_count, top_count, expert_count)
    flat_routes = routes.reshape(-1)
    onehot = (flat_routes[:, None] == jnp.arange(expert_count, dtype=jnp.int32)[None, :]).astype(
        jnp.int32
    )
    slot_ids = jnp.sum((jnp.cumsum(onehot, axis=0) - 1) * onehot, axis=1)
    target = flat_routes * slot_count + slot_ids
    placed = (
        target[None, :] == jnp.arange(expert_count * slot_count, dtype=jnp.int32)[:, None]
    ).astype(jnp.float32)
    chosen = jnp.sum(placed.reshape(expert_count * slot_count, seq_count, top_count), axis=2)
    outgoing = jnp.dot(
        chosen.astype(jnp.bfloat16), normal_ffn, preferred_element_type=jnp.float32
    ).astype(jnp.bfloat16)
    outgoing = outgoing.reshape(expert_count, slot_count, model_width)
    arrived = lax.all_to_all(outgoing, "ep", split_axis=0, concat_axis=0, tiled=True)
    outputs = swiglu(
        arrived.reshape(-1, model_width), expert_gate[0], expert_up[0], expert_down[0]
    ).astype(jnp.bfloat16)
    returned = lax.all_to_all(
        outputs.reshape(arrived.shape), "ep", split_axis=0, concat_axis=0, tiled=True
    )
    weights_by_slot = placed * route_weight.reshape(-1)[None, :]
    combine = jnp.sum(
        weights_by_slot.reshape(expert_count * slot_count, seq_count, top_count), axis=2
    )
    return lax.dot_general(
        combine, returned.reshape(-1, model_width).astype(jnp.float32), (((0,), (0,)), ((), ()))
    )


def per_device(
    tokens,
    lengths,
    cache_keys,
    cache_values,
    retention_state,
    mix_gain,
    query_weight,
    key_weight,
    value_weight,
    out_weight,
    ffn_gain,
    routes,
    route_scores,
    expert_gate,
    expert_up,
    expert_down,
    shared_gate,
    shared_up,
    shared_down,
    dense_gate,
    dense_up,
    dense_down,
    dense_mix,
):
    residual, new_keys, new_values = retain(
        tokens,
        lengths,
        mix_gain,
        query_weight,
        key_weight,
        value_weight,
        out_weight,
        cache_keys,
        cache_values,
        retention_state,
    )
    normal_ffn = (normed(residual) * ffn_gain).astype(jnp.bfloat16)
    shared_out = swiglu(normal_ffn, shared_gate, shared_up, shared_down)
    gated = jax.nn.sigmoid(dense_mix)
    route_weight = route_scores / jnp.sum(route_scores, axis=-1, keepdims=True) * route_scale
    pieces = side_by_side((dense_gate, dense_up, dense_down), "ep", 0, 1)
    dense_out = dense_part(normal_ffn, pieces[0], pieces[1], pieces[2])
    combined = (
        shared_out
        + gated * dense_out
        + exchanged_experts(normal_ffn, routes, route_weight, expert_gate, expert_up, expert_down)
    )
    layer_out = (residual + normed(combined)).astype(jnp.bfloat16)
    return (layer_out, new_keys, new_values)


def solution(mesh):
    in_specs = (
        P("ep", None),
        P("ep"),
        P("ep", None, None),
        P("ep", None, None),
        P("ep", None, None, None),
        P(),
        P(),
        P(),
        P(),
        P(),
        P(),
        P("ep", None),
        P("ep", None),
        P("ep", None, None),
        P("ep", None, None),
        P("ep", None, None),
        P(),
        P(),
        P(),
        P("ep", None),
        P("ep", None),
        P("ep", None),
        P(),
    )
    out_specs = (P("ep", None), P("ep", None), P("ep", None))
    return jax.shard_map(
        per_device, mesh=mesh, in_specs=in_specs, out_specs=out_specs, check_vma=False
    )
```

profile of v0, /device:TPU:1, one launch (start us, length us, event | category | flops | bytes accessed | tf_op | source)
XLA Modules:
  0.0 143.6 jit_solution(467105404568314871)
XLA Ops:
  7.2 1.7 %pad_maximum_fusion = bf16[32,3072]{1,0:T(8,128)(2,1)} fusion(bf16[32,1024]{1,0:T(8,128)(2,1)} %param.44, bf16[32,1024]{1,0:T(8,128)(2,1)} %param.43, bf16[32,1024]{1,0:T(8,128)(2,1)} %param.42), kind=kLoop, calls=%fused_computation.35 | loop fusion | flops 589824 | bytes 393216 | tf_op jit(solution)/shard_map/concatenate | solution.py:16
  9.0 0.9 fusion.41
  9.9 1.6 %fusion.67 = f32[16,512]{1,0:T(8,128)S(1)} fusion(bf16[1024,512]{1,0:T(8,128)(2,1)} %param.29, bf16[16,1024]{1,0:T(8,128)(2,1)} %param.23, f32[1024]{0:T(1024)} %param.28, f32[16]{0:T(128)S(1)} %add_rsqrt_fusion.4), kind=kOutput, calls=%fused_computation.108 | convolution fusion | flops 16842752 | bytes 1118272 | tf_op jit(solution)/shard_map/dot_general | solution.py:64
  11.5 0.7 convert_element_type.102
  12.2 1.5 %fusion.65 = f32[16,512]{1,0:T(8,128)S(1)} fusion(bf16[1024,512]{1,0:T(8,128)(2,1)} %param.30, bf16[16,1024]{1,0:T(8,128)(2,1)} %param.23, f32[1024]{0:T(1024)} %param.28, f32[16]{0:T(128)S(1)} %add_rsqrt_fusion.4), kind=kOutput, calls=%fused_computation.107 | convolution fusion | flops 16842752 | bytes 1118272 | tf_op jit(solution)/shard_map/dot_general | solution.py:67
  13.8 3.9 %copy.44 = bf16[16,128,512]{1,2,0:T(8,128)(2,1)} copy(bf16[16,128,512]{2,1,0:T(8,128)(2,1)} %param.25) | data formatting | bytes 4194304 | tf_op jit(solution)/shard_map/reshape | solution.py:79
  18.2 2.0 %convolution_convert_fusion.2 = bf16[16,1024]{1,0:T(8,128)(2,1)S(1)} fusion(bf16[1024,1024]{1,0:T(8,128)(2,1)} %param.31, bf16[16,1024]{1,0:T(8,128)(2,1)S(1)} %copy-done.1, f32[1024]{0:T(1024)S(1)} %copy-done.4, f32[16]{0:T(128)S(1)} %add_rsqrt_fusion.4), kind=kOutput, calls=%fused_computation.18 | convolution fusion | flops 33636352 | bytes 2166848 | tf_op jit(solution)/shard_map/dot_general | solution.py:70
  20.5 2.2 %fusion.50 = f32[16,4,1,128]{3,2,1,0:T(1,128)S(1)} fusion(bf16[16,128,4,128]{1,3,2,0:T(8,128)(2,1)} %bitcast.56, bf16[16,4,128,1]{2,1,0,3:T(4,128)(2,1)S(1)} %bitcast.58), kind=kOutput, calls=%fused_computation.72 | convolution fusion | flops 2097152 | bytes 2146304 | tf_op jit(solution)/shard_map/shd,sjhd->shj/dot_general | solution.py:81
  22.9 2.9 %fusion.12 = f32[16,4,1,256]{3,2,1,0:T(1,128)S(1)} fusion(bf16[16,16,4,8,256]{4,3,2,1,0:T(8,128)(2,1)} %bitcast.57, bf16[16,4,128,1]{2,1,0,3:T(4,128)(2,1)S(1)} %fusion.52), kind=kOutput, calls=%fused_computation.8 | convolution fusion | flops 4194304 | bytes 4276224 | tf_op jit(solution)/shard_map/shj,sjhe->she/dot_general | solution.py:92
  25.8 4.1 %fusion.48 = f32[16,4,1,256]{3,2,1,0:T(1,128)S(1)} fusion(f32[16,4,128,256]{3,2,1,0:T(8,128)} %param.27, bf16[16,4,128,1]{2,1,0,3:T(4,128)(2,1)S(1)} %bitcast.59), kind=kOutput, calls=%fused_computation.70 | convolution fusion | flops 4194304 | bytes 8470528 | tf_op jit(solution)/shard_map/shd,shde->she/dot_general | solution.py:96
  31.0 0.7 convert_reduce_fusion
  31.7 0.5 multiply_reduce_fusion.2
  32.2 0.2 multiply_reduce_fusion.1
  32.5 0.3 convolution_convert_fusion.1
  32.9 0.2 reshape.268
  33.1 29.4 %all_to_all.10 = bf16[128,2,1024]{2,1,0:T(2,128)(2,1)} all-to-all(bf16[128,2,1024]{2,1,0:T(2,128)(2,1)S(1)} %reshape.268), channel_id=1, replica_groups=mesh['ep'=128] {'ep'}, dimensions={0} | all-to-all | bytes 1048576 | tf_op jit(solution)/shard_map/all_to_all | solution.py:136
  62.5 1.2 reshape.269
  63.7 1.3 fusion.27
  65.1 1.9 %convolution_convert_fusion = bf16[256,1024]{1,0:T(8,128)(2,1)S(1)} fusion(bf16[256,1024]{1,0:T(8,128)(2,1)S(1)} %reshape.269, bf16[1,256,1024]{2,1,0:T(8,128)(2,1)} %param.38, bf16[1,1024,256]{2,1,0:T(8,128)(2,1)} %param.37, f32[256,256]{1,0:T(8,128)S(1)} %fusion.27), kind=kOutput, calls=%fused_computation.11 | convolution fusion | flops 269090816 | bytes 2359296 | tf_op jit(solution)/shard_map/dot_general | solution.py:46
  67.0 1.0 reshape.270
  68.1 5.6 %all-to-all-start.1 = ((bf16[128,2,1024]{2,1,0:T(2,128)(2,1)}), bf16[128,2,1024]{2,1,0:T(2,128)(2,1)S(1)}, u32[]{:S(2)}, u32[]{:S(2)}) async-start(bf16[128,2,1024]{2,1,0:T(2,128)(2,1)} %reshape.270), calls=%async_computation.1 | async-start | bytes 1048576 | tf_op jit(solution)/shard_map/all_to_all | solution.py:140
  73.7 0.6 copy.63
  74.3 1.3 add_divide_fusion
  75.6 1.2 fusion.71
  76.8 16.5 %all-to-all-done.1 = bf16[128,2,1024]{2,1,0:T(2,128)(2,1)S(1)} async-done(((bf16[128,2,1024]{2,1,0:T(2,128)(2,1)}), bf16[128,2,1024]{2,1,0:T(2,128)(2,1)S(1)}, u32[]{:S(2)}, u32[]{:S(2)}) %all-to-all-start.1) | async-done | bytes 524320 | tf_op jit(solution)/shard_map/all_to_all | solution.py:140
  93.3 0.2 reshape.271
  93.5 23.9 %all-gather.2.cloned.1.call-done = bf16[4096,3072]{1,0:T(8,128)(2,1)} async-done(((bf16[32,3072]{1,0:T(8,128)(2,1)}), bf16[4096,3072]{1,0:T(8,128)(2,1)}) %all-gather.2.cloned.1.call-update) | async-done | bytes 25165840 | tf_op jit(solution)/shard_map/all_gather | solution.py:17
  117.4 5.7 %fusion.4 = f32[16,4096]{1,0:T(8,128)S(1)} fusion(bf16[16,1024]{1,0:T(8,128)(2,1)S(1)} %multiply_convert_fusion, bf16[4096,3072]{1,0:T(8,128)(2,1)} %all-gather.2.cloned.1.call-done), kind=kOutput, calls=%fused_computation.4 | convolution fusion | flops 134217728 | bytes 8683520 | tf_op jit(solution)/shard_map/dot_general | solution.py:51
  123.1 9.9 %fusion.18 = f32[16,1024]{1,0:T(8,128)} fusion(bf16[4096,3072]{1,0:T(8,128)(2,1)} %all-gather.2.cloned.1.call-done, bf16[16,1024]{1,0:T(8,128)(2,1)S(1)} %multiply_convert_fusion, f32[16,4096]{1,0:T(8,128)S(1)} %fusion.4, f32[1024]{0:T(1024)} %add_divide_fusion), kind=kOutput, calls=%fused_computation.17 | convolution fusion | flops 268845056 | bytes 17141760 | tf_op jit(solution)/shard_map/dot_general | solution.py:54
  132.9 1.5 %convolution_add_fusion.1 = f32[16,1024]{1,0:T(8,128)S(1)} fusion(f32[16,1024]{1,0:T(8,128)} %fusion.18, bf16[256,1024]{1,0:T(8,128)(2,1)S(1)} %copy-done.2, bf16[16,1024]{1,0:T(8,128)(2,1)S(1)} %multiply_convert_fusion, bf16[1024,256]{1,0:T(8,128)(2,1)} %param.40, f32[16,256]{1,0:T(8,128)S(1)} %fusion.71), kind=kOutput, calls=%fused_computation.16 | convolution fusion | flops 16818176 | bytes 1228800 | tf_op jit(solution)/shard_map/dot_general | solution.py:46
  134.4 1.0 multiply_reduce_fusion
  135.4 1.3 add_convert_fusion
  (56 shorter events, 2.2 us)
Async XLA Ops:
  7.2 24.6 %copy-start = (bf16[1024,1024]{1,0:T(8,128)(2,1)S(1)}, bf16[1024,1024]{1,0:T(8,128)(2,1)}, u32[]{:S(2)}) copy-start(bf16[1024,1024]{1,0:T(8,128)(2,1)} %param.32) | copy-start | bytes 6291460
  7.2 11.0 %copy-start.1 = (bf16[16,1024]{1,0:T(8,128)(2,1)S(1)}, bf16[16,1024]{1,0:T(8,128)(2,1)}, u32[]{:S(2)}) copy-start(bf16[16,1024]{1,0:T(8,128)(2,1)} %param.23) | copy-start | bytes 98308
  7.2 11.0 %copy-start.4 = (f32[1024]{0:T(1024)S(1)}, f32[1024]{0:T(1024)}, u32[]{:S(2)}) copy-start(f32[1024]{0:T(1024)} %param.28) | copy-start | bytes 12292
  7.2 110.2 %all-gather.2.cloned.1.call-start = ((), (), s32[]{:S(2)}) async-start(), calls=%async_computation.2 | async-start | bytes 25362432 | tf_op jit(solution)/shard_map/all_gather | solution.py:17
  11.5 8.9 %copy-start.9 = (s32[16]{0:T(128)S(1)}, s32[16]{0:T(128)}, u32[]{:S(2)}) copy-start(s32[16]{0:T(128)} %param.24) | copy-start | bytes 196
  20.2 2.7 %copy-start.3 = (bf16[16,1024]{1,0:T(8,128)(2,1)}, bf16[16,1024]{1,0:T(8,128)(2,1)S(1)}, u32[]{:S(2)}) copy-start(bf16[16,1024]{1,0:T(8,128)(2,1)S(1)} %convolution_convert_fusion.2) | copy-start | bytes 98308
  25.8 4.4 %copy-start.5 = (s32[16,6]{0,1:T(8,128)S(1)}, s32[16,6]{0,1:T(8,128)}, u32[]{:S(2)}) copy-start(s32[16,6]{0,1:T(8,128)} %param.34) | copy-start | bytes 1156
  25.8 5.1 %copy-start.6 = (f32[16,6]{0,1:T(8,128)S(1)}, f32[16,6]{0,1:T(8,128)}, u32[]{:S(2)}) copy-start(f32[16,6]{0,1:T(8,128)} %param.35) | copy-start | bytes 1156
  25.8 6.6 %copy-start.8 = (f32[1024]{0:T(1024)S(1)}, f32[1024]{0:T(1024)}, u32[]{:S(2)}) copy-start(f32[1024]{0:T(1024)} %param.33) | copy-start | bytes 12292
  32.2 30.3 %copy-start.7 = (f32[16]{0:T(128)}, f32[16]{0:T(128)S(1)}, u32[]{:S(2)}) copy-start(f32[16]{0:T(128)S(1)} %add_rsqrt_fusion.3) | copy-start | bytes 196
  68.1 25.2 %all-to-all-start.1 = ((bf16[128,2,1024]{2,1,0:T(2,128)(2,1)}), bf16[128,2,1024]{2,1,0:T(2,128)(2,1)S(1)}, u32[]{:S(2)}, u32[]{:S(2)}) async-start(bf16[128,2,1024]{2,1,0:T(2,128)(2,1)} %reshape.270), calls=%async_computation.1 | async-start | bytes 1048576 | tf_op jit(solution)/shard_map/all_to_all | solution.py:140
  123.1 9.9 %copy-start.2 = (bf16[256,1024]{1,0:T(8,128)(2,1)S(1)}, bf16[256,1024]{1,0:T(8,128)(2,1)}, u32[]{:S(2)}) copy-start(bf16[256,1024]{1,0:T(8,128)(2,1)} %param.41) | copy-start | bytes 1572868
Sparse Core Ops, SparseCore 0:
  11.1 106.2 all-gather.1
where the time goes:
time: 144 us
  waiting for transfers between devices  40.4 us (28%)
  matrix products  37.7 us (26%)
  blocking collectives  29.4 us (20%)
  between operations  14.3 us (10%)
  other arithmetic  8.52 us (6%)
  local copies, waits for them, and re-layouts  7.67 us (5%)
  starting transfers between devices  5.61 us (4%)
    all_to_all x1, blocking collectives, exchanged_experts(): lax.all_to_all(outgoing, 'ep', split_axis=0, concat_axis=0, tiled=True)  29.4 us
    all_gather x1, waiting for transfers between devices, side_by_side(): lax.all_gather(both, axis, axis=dim, tiled=True)  23.9 us
    all_to_all x1, waiting for transfers between devices, exchanged_experts(): lax.all_to_all(outputs.reshape(arrived.shape), 'ep', split_axis=0, concat...  16.5 us
    dot_general x1, matrix products, dense_part(): return jnp.dot(hidden, down_rows, preferred_element_type=jnp.float32)  9.86 us
    dot_general x1, matrix products, dense_part(): lax.dot_general(inputs, gate_rows, contract, preferred_element_type=jnp.f...  5.65 us
    all_to_all x1, starting transfers between devices, exchanged_experts(): lax.all_to_all(outputs.reshape(arrived.shape), 'ep', split_axis=0, concat...  5.58 us
    dot_general x1, matrix products, retain(): jnp.einsum('shd,shde->she', queries.astype(jnp.float32), carry_state)  4.06 us
    reshape x1, local copies, waits for them, and re-layouts, retain(): cache_keys.reshape(seq_count, block_size, head_count, key_size)  3.91 us
  transfers between devices with their start and end apart: 2, of which 2 were waited for; matrix products, arithmetic and copies ran while one was open for 23% of the time, Pallas kernels for 0%

commit v1 on v0

--- a/solution.py
+++ b/solution.py
@@ -1,20 +1,23 @@
+import functools
+
 import jax
 import jax.numpy as jnp
 from jax import lax
+from jax.experimental import pallas as pl
+from jax.experimental.pallas import tpu as pltpu
 from jax.sharding import PartitionSpec as P
 
 eps = 1e-06
 route_scale = 2.5
 rope_base = 10000.0
-
-
-def side_by_side(arrays, axis, dim, along):
-    ends, at = ([], 0)
-    for a in arrays[:-1]:
-        at += a.shape[along]
-        ends.append(at)
-    both = jnp.concatenate(arrays, axis=along)
-    return tuple(jnp.split(lax.all_gather(both, axis, axis=dim, tiled=True), ends, axis=along))
+MESH = pl.DeviceIdType.MESH
+F32 = jnp.float32
+BF16 = jnp.bfloat16
+N_DEV = 128
+TOKENS = 16
+WIDTH = 1024
+TOP = 6
+STEP = 53
 
 
 def normed(values):
@@ -37,21 +40,6 @@
         [first_half * cosine - second * sine_part, first_half * sine_part + second * cosine],
         axis=-1,
     )
-
-
-def swiglu(inputs, w_gate, w_up, w_down):
-    gate_part = jnp.dot(inputs, w_gate, preferred_element_type=jnp.float32)
-    up_part = jnp.dot(inputs, w_up, preferred_element_type=jnp.float32)
-    hidden = (jax.nn.silu(gate_part) * up_part).astype(jnp.bfloat16)
-    return jnp.dot(hidden, w_down, preferred_element_type=jnp.float32)
-
-
-def dense_part(inputs, gate_rows, up_rows, down_rows):
-    contract = (((1,), (1,)), ((), ()))
-    gate_part = lax.dot_general(inputs, gate_rows, contract, preferred_element_type=jnp.float32)
-    up_part = lax.dot_general(inputs, up_rows, contract, preferred_element_type=jnp.float32)
-    hidden = (jax.nn.silu(gate_part) * up_part).astype(jnp.bfloat16)
-    return jnp.dot(hidden, down_rows, preferred_element_type=jnp.float32)
 
 
 def retain(
@@ -110,43 +98,358 @@
     )
 
 
-def capacity(seq_count, top_count, expert_count):
-    return max(2, seq_count * top_count * 8 // (3 * expert_count))
-
-
-def exchanged_experts(normal_ffn, routes, route_weight, expert_gate, expert_up, expert_down):
-    seq_count, top_count = routes.shape
-    model_width = normal_ffn.shape[1]
-    expert_count = lax.axis_size("ep") * expert_gate.shape[0]
-    slot_count = capacity(seq_count, top_count, expert_count)
-    flat_routes = routes.reshape(-1)
-    onehot = (flat_routes[:, None] == jnp.arange(expert_count, dtype=jnp.int32)[None, :]).astype(
-        jnp.int32
-    )
-    slot_ids = jnp.sum((jnp.cumsum(onehot, axis=0) - 1) * onehot, axis=1)
-    target = flat_routes * slot_count + slot_ids
-    placed = (
-        target[None, :] == jnp.arange(expert_count * slot_count, dtype=jnp.int32)[:, None]
-    ).astype(jnp.float32)
-    chosen = jnp.sum(placed.reshape(expert_count * slot_count, seq_count, top_count), axis=2)
-    outgoing = jnp.dot(
-        chosen.astype(jnp.bfloat16), normal_ffn, preferred_element_type=jnp.float32
-    ).astype(jnp.bfloat16)
-    outgoing = outgoing.reshape(expert_count, slot_count, model_width)
-    arrived = lax.all_to_all(outgoing, "ep", split_axis=0, concat_axis=0, tiled=True)
-    outputs = swiglu(
-        arrived.reshape(-1, model_width), expert_gate[0], expert_up[0], expert_down[0]
-    ).astype(jnp.bfloat16)
-    returned = lax.all_to_all(
-        outputs.reshape(arrived.shape), "ep", split_axis=0, concat_axis=0, tiled=True
-    )
-    weights_by_slot = placed * route_weight.reshape(-1)[None, :]
-    combine = jnp.sum(
-        weights_by_slot.reshape(expert_count * slot_count, seq_count, top_count), axis=2
-    )
-    return lax.dot_general(
-        combine, returned.reshape(-1, model_width).astype(jnp.float32), (((0,), (0,)), ((), ()))
-    )
+def dot(a, b):
+    return jnp.dot(a, b, preferred_element_type=F32)
+
+
+def dot_t(a, b):
+    return lax.dot_general(a, b, (((1,), (1,)), ((), ())), preferred_element_type=F32)
+
+
+def dot_0(a, b):
+    return lax.dot_general(a, b, (((0,), (0,)), ((), ())), preferred_element_type=F32)
+
+
+def silu(v):
+    return v / (1.0 + jnp.exp(-v))
+
+
+def iota(shape, dim):
+    return lax.broadcasted_iota(jnp.int32, shape, dim)
+
+
+def one_hot(mask):
+    return jnp.where(mask, 1.0, 0.0).astype(BF16)
+
+
+def build_routing(routes_ref, scores_ref, place_ref, comb_ref):
+    routes = routes_ref[...].astype(F32)
+    scores = scores_ref[...]
+    weight = scores / jnp.sum(scores, axis=-1, keepdims=True) * route_scale
+    spread = one_hot((iota((TOKENS, 128), 1) & 15) == iota((TOKENS, 128), 0))
+    spread_t = one_hot((iota((128, TOKENS), 0) & 15) == iota((128, TOKENS), 1))
+    eye = one_hot(iota((128, 128), 0) == iota((128, 128), 1))
+    lanes = dot_0(routes.astype(BF16), spread)
+    earlier = iota((TOKENS, 128), 0) < (iota((TOKENS, 128), 1) & 15)
+    ranks = []
+    for j in range(TOP):
+        hits = jnp.zeros((TOKENS, 128), F32)
+        for i in range(TOP):
+            same = routes[:, i : i + 1] == lanes[j : j + 1, :]
+            hits = hits + jnp.where(same & earlier, 1.0, 0.0)
+        ranks.append(jnp.sum(hits, axis=0, keepdims=True))
+    rank = jnp.concatenate(ranks, axis=0)
+    chunk_lane = (iota((TOP, 128), 1) >> 4).astype(F32)
+    code = lanes * 16.0 + chunk_lane * 2.0 + rank
+    columns = dot(spread_t, routes.astype(BF16))
+    rank_columns = dot_t(eye, rank.astype(BF16))
+    weight_columns = dot(spread_t, weight.astype(BF16))
+    code_t = columns * 16.0 + (iota((128, TOP), 0) >> 4).astype(F32) * 2.0 + rank_columns
+
+    def place_rows(b, carry):
+        at = pl.multiple_of(b * 128, 128)
+        row = (iota((128, 128), 0) + at).astype(F32)
+        found = row == code[0:1, :]
+        for j in range(1, TOP):
+            found = found | (row == code[j : j + 1, :])
+        place_ref[pl.ds(at, 128), :] = one_hot(found)
+        lane = (iota((128, 128), 1) + at).astype(F32)
+        mixed = jnp.zeros((128, 128), F32)
+        for j in range(TOP):
+            mixed = jnp.where(lane == code_t[:, j : j + 1], weight_columns[:, j : j + 1], mixed)
+        comb_ref[:, pl.ds(at, 128)] = mixed.astype(BF16)
+        return carry
+
+    lax.fori_loop(0, N_DEV * 16 // 128, place_rows, 0)
+
+
+def layer_kernel(
+    nf_ref,
+    residual_ref,
+    routes_ref,
+    scores_ref,
+    mix_ref,
+    eg_ref,
+    eu_ref,
+    ed_ref,
+    sg_ref,
+    su_ref,
+    sd_ref,
+    dg_ref,
+    du_ref,
+    dd_ref,
+    out_ref,
+    place,
+    comb,
+    eg,
+    eu,
+    ed,
+    sg,
+    su,
+    sd,
+    dw,
+    nf,
+    snd,
+    rcv,
+    snd2,
+    rcv2,
+    acts,
+    part,
+    parts,
+    rows,
+    load_sem,
+    dense_load_sem,
+    dw_send,
+    dw_recv,
+    fw_send,
+    fw_recv,
+    a2a_sem,
+    ret_sem,
+    act_sem,
+    part_sem,
+):
+    me = lax.axis_index("ep")
+    lane8 = lax.rem(me, 8)
+    group = lax.div(me, 8)
+    core = lax.rem(me, 2)
+    base8 = group * 8
+    sibling = me + 1 - 2 * core
+
+    barrier = pltpu.get_barrier_semaphore()
+
+    def greet(i, carry):
+        peer = lax.rem(me + i, N_DEV)
+        pl.semaphore_signal(barrier, inc=1, device_id=(peer,), device_id_type=MESH)
+        return carry
+
+    lax.fori_loop(1, N_DEV, greet, 0)
+
+    own_rows = pl.ds(pl.multiple_of(lane8 * 32, 32), 32)
+    own_loads = [
+        pltpu.make_async_copy(src, dw.at[i, own_rows], dense_load_sem.at[i])
+        for i, src in enumerate((dg_ref, du_ref, dd_ref))
+    ]
+    for c in own_loads:
+        c.start()
+    loads = [
+        pltpu.make_async_copy(src, dst, load_sem.at[i])
+        for i, (src, dst) in enumerate(
+            (
+                (sg_ref, sg),
+                (su_ref, su),
+                (sd_ref, sd),
+                (eg_ref.at[0], eg),
+                (eu_ref.at[0], eu),
+                (ed_ref.at[0], ed),
+            )
+        )
+    ]
+    for c in loads:
+        c.start()
+
+    build_routing(routes_ref, scores_ref, place, comb)
+
+    for c in own_loads:
+        c.wait()
+    pl.semaphore_wait(barrier, N_DEV - 1)
+
+    def shard(slot):
+        return dw.at[:, pl.ds(pl.multiple_of(slot * 32, 32), 32), :]
+
+    weight_sends = []
+    for i in range(4):
+        peer = sibling if i == 0 else base8 + lax.rem(lane8 + 2 * i, 8)
+        weight_sends.append(
+            pltpu.make_async_remote_copy(
+                shard(lane8), shard(lane8), dw_send.at[i], dw_recv.at[i],
+                device_id=(peer,), device_id_type=MESH,
+            )
+        )
+    nf_value = nf_ref[...]
+    nf[...] = nf_value
+    stacked = jnp.concatenate([nf_value[:, k * 128 : (k + 1) * 128] for k in range(8)], axis=0)
+
+    def pack(b, carry):
+        at = pl.ds(pl.multiple_of(b * 256, 256), 256)
+        snd[at, :] = dot(place[at, :], stacked).astype(BF16)
+        return carry
+
+    lax.fori_loop(0, 8, pack, 0)
+
+    def tile(ref, index):
+        return ref.at[pl.ds(pl.multiple_of(index * 16, 16), 16), :]
+
+    def exchange(source, target, sems):
+        def send(i, carry):
+            peer = lax.rem(me + i * STEP, N_DEV)
+            pltpu.make_async_remote_copy(
+                tile(source, peer), tile(target, me), sems.at[0], sems.at[1],
+                device_id=(peer,), device_id_type=MESH,
+            ).start()
+            return carry
+
+        lax.fori_loop(1, N_DEV, send, 0)
+        own = pl.ds(pl.multiple_of(me * 16, 16), 16)
+        target[own, :] = source[own, :]
+
+    def all_tiles(source, target, sems):
+        whole = pl.ds(0, (N_DEV - 1) * 16)
+        return pltpu.make_async_remote_copy(
+            source.at[whole, :], target.at[whole, :], sems.at[0], sems.at[1],
+            device_id=(sibling,), device_id_type=MESH,
+        )
+
+    exchange(snd, rcv, a2a_sem)
+
+    act_rows = pl.ds(pl.multiple_of(group * 16, 16), 16)
+
+    def send_acts(i, carry):
+        peer = lax.rem(group + i, 16) * 8 + lane8
+        pltpu.make_async_remote_copy(
+            nf, acts.at[act_rows, :], act_sem.at[0], act_sem.at[1],
+            device_id=(peer,), device_id_type=MESH,
+        ).start()
+        return carry
+
+    lax.fori_loop(1, 16, send_acts, 0)
+    acts[act_rows, :] = nf_value
+    for c in weight_sends:
+        c.start()
+
+    for c in loads[:3]:
+        c.wait()
+    hidden = (silu(dot(nf_value, sg[...])) * dot(nf_value, su[...])).astype(BF16)
+    shared_out = dot(hidden, sd[...])
+
+    rowi = iota((256, 256), 0)
+    coli = iota((256, 256), 1)
+    swap = one_hot(coli == ((rowi >> 1) & 15) * 16 + (rowi >> 5) * 2 + (rowi & 1))
+    swap_t = one_hot(rowi == ((coli >> 1) & 15) * 16 + (coli >> 5) * 2 + (coli & 1))
+
+    for c in loads[3:]:
+        c.wait()
+    all_tiles(snd, rcv, a2a_sem).wait_recv()
+    for b in range(8):
+        moved = dot(swap, rcv[b * 256 : (b + 1) * 256, :]).astype(BF16)
+        for k in range(8):
+            rows[b * 32 : (b + 1) * 32, k * 128 : (k + 1) * 128] = moved[k * 32 : (k + 1) * 32, :]
+    taken = rows[...]
+    hidden = (silu(dot(taken, eg[...])) * dot(taken, eu[...])).astype(BF16)
+    rows[...] = dot(hidden, ed[...]).astype(BF16)
+    for b in range(8):
+        piece = rows[b * 32 : (b + 1) * 32, :]
+        column = jnp.concatenate([piece[:, k * 128 : (k + 1) * 128] for k in range(8)], axis=0)
+        snd2[b * 256 : (b + 1) * 256, :] = dot(swap_t, column).astype(BF16)
+    exchange(snd2, rcv2, ret_sem)
+
+    forwards = []
+    for i in range(1, 4):
+        slot = lax.rem(lane8 + 8 - 2 * i, 8)
+        pltpu.make_async_remote_copy(
+            shard(lane8), shard(slot), dw_send.at[i], dw_recv.at[i],
+            device_id=(sibling,), device_id_type=MESH,
+        ).wait_recv()
+        c = pltpu.make_async_remote_copy(
+            shard(slot), shard(slot), fw_send.at[i - 1], fw_recv.at[i - 1],
+            device_id=(sibling,), device_id_type=MESH,
+        )
+        c.start()
+        forwards.append(c)
+    for c in forwards:
+        c.wait_recv()
+    weight_sends[0].wait_recv()
+    pltpu.make_async_remote_copy(
+        acts.at[pl.ds(0, 240), :], acts.at[pl.ds(0, 240), :], act_sem.at[0], act_sem.at[1],
+        device_id=(sibling,), device_id_type=MESH,
+    ).wait_recv()
+    every = acts[...]
+    hidden = (silu(dot_t(every, dw[0])) * dot_t(every, dw[1])).astype(BF16)
+    part[...] = dot(hidden, dw[2]).astype(BF16)
+
+    def send_parts(i, carry):
+        to = lax.rem(group + i, 16)
+        pltpu.make_async_remote_copy(
+            tile(part, to), tile(parts, group), part_sem.at[0], part_sem.at[1],
+            device_id=(to * 8 + lane8,), device_id_type=MESH,
+        ).start()
+        return carry
+
+    lax.fori_loop(1, 16, send_parts, 0)
+    parts[act_rows, :] = part[act_rows, :]
+
+    all_tiles(snd2, rcv2, ret_sem).wait_recv()
+    mixed = dot(comb[...], rcv2[...])
+    routed = jnp.concatenate([mixed[k * 16 : (k + 1) * 16, :] for k in range(8)], axis=1)
+    gate = 1.0 / (1.0 + jnp.exp(-mix_ref[...]))
+
+    all_parts = pltpu.make_async_remote_copy(
+        part.at[pl.ds(0, 240), :], parts.at[pl.ds(0, 240), :], part_sem.at[0], part_sem.at[1],
+        device_id=(sibling,), device_id_type=MESH,
+    )
+    all_parts.wait_recv()
+    dense = parts[0:16, :].astype(F32)
+    for g in range(1, 16):
+        dense = dense + parts[g * 16 : (g + 1) * 16, :].astype(F32)
+    combined = shared_out + routed + gate * dense
+    out_ref[...] = (residual_ref[...] + normed(combined)).astype(BF16)
+
+    for c in weight_sends:
+        c.wait_send()
+    for c in forwards:
+        c.wait_send()
+    all_tiles(snd, rcv, a2a_sem).wait_send()
+    all_tiles(snd2, rcv2, ret_sem).wait_send()
+    for sems in (act_sem,):
+        pltpu.make_async_remote_copy(
+            acts.at[pl.ds(0, 240), :], acts.at[pl.ds(0, 240), :], sems.at[0], sems.at[1],
+            device_id=(sibling,), device_id_type=MESH,
+        ).wait_send()
+    all_parts.wait_send()
+
+
+def run_layer(nf, residual, routes, scores, mix, eg, eu, ed, sg, su, sd, dg, du, dd):
+    vmem = pl.BlockSpec(memory_space=pltpu.VMEM)
+    anywhere = pl.BlockSpec(memory_space=pl.ANY)
+    dma = pltpu.SemaphoreType.DMA
+    slots = (N_DEV * 16, 128)
+    return pl.pallas_call(
+        layer_kernel,
+        name="layer",
+        out_shape=jax.ShapeDtypeStruct((TOKENS, WIDTH), BF16),
+        in_specs=[vmem] * 5 + [anywhere] * 9,
+        out_specs=vmem,
+        scratch_shapes=[
+            pltpu.VMEM(slots, BF16),
+            pltpu.VMEM((128, N_DEV * 16), BF16),
+            pltpu.VMEM((1024, 256), BF16),
+            pltpu.VMEM((1024, 256), BF16),
+            pltpu.VMEM((256, 1024), BF16),
+            pltpu.VMEM((1024, 256), BF16),
+            pltpu.VMEM((1024, 256), BF16),
+            pltpu.VMEM((256, 1024), BF16),
+            pltpu.VMEM((3, 256, 1024), BF16),
+            pltpu.VMEM((TOKENS, WIDTH), BF16),
+            pltpu.VMEM(slots, BF16),
+            pltpu.VMEM(slots, BF16),
+            pltpu.VMEM(slots, BF16),
+            pltpu.VMEM(slots, BF16),
+            pltpu.VMEM((256, 1024), BF16),
+            pltpu.VMEM((256, 1024), BF16),
+            pltpu.VMEM((256, 1024), BF16),
+            pltpu.VMEM((256, 1024), BF16),
+            dma((6,)),
+            dma((3,)),
+            dma((4,)),
+            dma((4,)),
+            dma((3,)),
+            dma((3,)),
+            dma((2,)),
+            dma((2,)),
+            dma((2,)),
+            dma((2,)),
+        ],
+        compiler_params=pltpu.CompilerParams(collective_id=0, has_side_effects=True),
+    )(nf, residual, routes, scores, mix, eg, eu, ed, sg, su, sd, dg, du, dd)
 
 
 def per_device(
@@ -187,17 +490,22 @@
         retention_state,
     )
     normal_ffn = (normed(residual) * ffn_gain).astype(jnp.bfloat16)
-    shared_out = swiglu(normal_ffn, shared_gate, shared_up, shared_down)
-    gated = jax.nn.sigmoid(dense_mix)
-    route_weight = route_scores / jnp.sum(route_scores, axis=-1, keepdims=True) * route_scale
-    pieces = side_by_side((dense_gate, dense_up, dense_down), "ep", 0, 1)
-    dense_out = dense_part(normal_ffn, pieces[0], pieces[1], pieces[2])
-    combined = (
-        shared_out
-        + gated * dense_out
-        + exchanged_experts(normal_ffn, routes, route_weight, expert_gate, expert_up, expert_down)
-    )
-    layer_out = (residual + normed(combined)).astype(jnp.bfloat16)
+    layer_out = run_layer(
+        normal_ffn,
+        residual,
+        routes,
+        route_scores,
+        dense_mix[None, :],
+        expert_gate,
+        expert_up,
+        expert_down,
+        shared_gate,
+        shared_up,
+        shared_down,
+        dense_gate,
+        dense_up,
+        dense_down,
+    )
     return (layer_out, new_keys, new_values)
 
 

time: 144 us -> 68.4 us (0.48)
  Pallas kernels: 0 us -> 42.8 us
  waiting for transfers between devices: 40.4 us -> 0 us
  blocking collectives: 29.4 us -> 0 us
  matrix products: 37.7 us -> 13.3 us
  between operations: 14.3 us -> 0.84 us
  starting transfers between devices: 5.61 us -> 0 us
  other arithmetic: 8.52 us -> 3.73 us
    pallas_call x0 -> x1, Pallas kernels: none -> 42.8 us  [run_layer(): pl.pallas_call(layer_kernel, name='layer', out_shape=jax.ShapeDtypeStruct...]
    all_to_all x1 -> x0, blocking collectives: 29.4 us -> none  [exchanged_experts(): lax.all_to_all(outgoing, 'ep', split_axis=0, concat_axis=0, tiled=True)]
    all_gather x1 -> x0, waiting for transfers between devices: 23.9 us -> none  [side_by_side(): lax.all_gather(both, axis, axis=dim, tiled=True)]
    dot_general x8 -> x0, matrix products: 22.8 us -> none  [the longest x1 9.86 us: dense_part(): return jnp.dot(hidden, down_rows, preferred_element_type=jnp.float32)]
    all_to_all x1 -> x0, waiting for transfers between devices: 16.5 us -> none  [exchanged_experts(): lax.all_to_all(outputs.reshape(arrived.shape), 'ep', split_axis=0, concat...]
    all_to_all x1 -> x0, starting transfers between devices: 5.58 us -> none  [exchanged_experts(): lax.all_to_all(outputs.reshape(arrived.shape), 'ep', split_axis=0, concat...]
    reshape x4 -> x0, local copies, waits for them, and re-layouts: 2.68 us -> none  [the longest x1 1.24 us: exchanged_experts(): arrived.reshape(-1, model_width)]
    unnamed x23 -> x25, local copies, waits for them, and re-layouts: 0.75 us -> 3.4 us
  transfers between devices with their start and end apart: 2 -> 0, of which waited for: 2 -> 0; matrix products, arithmetic and copies ran while one was open for 23% -> 0% of each run, Pallas kernels for 0% -> 0%
where the time goes in v1:
time: 68.4 us; the launch traced here: 68 us
  Pallas kernels  42.8 us (63%)
  matrix products  13.3 us (19%)
  local copies, waits for them, and re-layouts  7.38 us (11%)
  other arithmetic  3.73 us (5%)
  between operations  0.84 us (1%)
    pallas_call x1, Pallas kernels, run_layer(): pl.pallas_call(layer_kernel, name='layer', out_shape=jax.ShapeDtypeStruct...  42.8 us
    dot_general x1, matrix products, retain(): jnp.einsum('shd,shde->she', queries.astype(jnp.float32), carry_state)  4.19 us
    reshape x1, local copies, waits for them, and re-layouts, retain(): cache_keys.reshape(seq_count, block_size, head_count, key_size)  3.91 us
    unnamed x25, local copies, waits for them, and re-layouts  3.4 us
    dot_general x1, matrix products, retain(): jnp.einsum('shj,sjhe->she', weighted, stored_values, preferred_element_ty...  2.84 us
    dot_general x1, matrix products, retain(): jnp.einsum('shd,sjhd->shj', queries, stored_keys, preferred_element_type=...  2.24 us
    dot_general x1, matrix products, retain(): jnp.dot(normal_in, w_query, preferred_element_type=jnp.float32)  1.55 us
    dot_general x1, matrix products, retain(): jnp.dot(normal_in, w_key, preferred_element_type=jnp.float32)  1.55 us

profile of v1, /device:TPU:1, one launch (start us, length us, event | category | flops | bytes accessed | tf_op | source)
XLA Modules:
  0.0 68.0 jit_solution(13370391582107674164)
XLA Ops:
  0.6 0.0 copy-start
  0.6 1.0 %fusion.3 = f32[16]{0:T(128)S(1)} fusion(bf16[16,1024]{1,0:T(8,128)(2,1)} %param.23), kind=kLoop, calls=%fused_computation.7 | loop fusion | flops 49136 | bytes 32832 | tf_op jit(solution)/shard_map/reduce_sum | solution.py:24
  1.7 1.6 %fusion.18 = f32[16,512]{1,0:T(8,128)S(1)} fusion(bf16[1024,512]{1,0:T(8,128)(2,1)} %param.29, bf16[16,1024]{1,0:T(8,128)(2,1)} %param.23, f32[1024]{0:T(1024)} %param.28, f32[16]{0:T(128)S(1)} %add_rsqrt_fusion.3), kind=kOutput, calls=%fused_computation.52 | convolution fusion | flops 16842752 | bytes 1118272 | tf_op jit(solution)/shard_map/dot_general | solution.py:52
  3.3 0.7 convert_element_type.73
  3.9 0.1 multiply_cosine_fusion
  4.1 0.1 multiply_subtract_fusion.1
  4.1 1.5 %fusion.16 = f32[16,512]{1,0:T(8,128)S(1)} fusion(bf16[1024,512]{1,0:T(8,128)(2,1)} %param.30, bf16[16,1024]{1,0:T(8,128)(2,1)} %param.23, f32[1024]{0:T(1024)} %param.28, f32[16]{0:T(128)S(1)} %add_rsqrt_fusion.3), kind=kOutput, calls=%fused_computation.51 | convolution fusion | flops 16842752 | bytes 1118272 | tf_op jit(solution)/shard_map/dot_general | solution.py:55
  5.7 0.1 multiply_subtract_fusion
  5.8 0.2 multiply_reduce_fusion.3
  6.0 3.9 %copy.35 = bf16[16,128,512]{1,2,0:T(8,128)(2,1)} copy(bf16[16,128,512]{2,1,0:T(8,128)(2,1)} %param.25) | data formatting | bytes 4194304 | tf_op jit(solution)/shard_map/reshape | solution.py:67
  9.9 2.2 %fusion.11 = f32[16,4,1,128]{3,2,1,0:T(1,128)S(1)} fusion(bf16[16,128,4,128]{1,3,2,0:T(8,128)(2,1)} %bitcast.34, bf16[16,4,128,1]{2,1,0,3:T(4,128)(2,1)S(1)} %bitcast.36), kind=kOutput, calls=%fused_computation.30 | convolution fusion | flops 2097152 | bytes 2146304 | tf_op jit(solution)/shard_map/shd,sjhd->shj/dot_general | solution.py:69
  12.2 0.1 maximum_convert_fusion.1
  12.3 0.1 iota_compare_fusion
  12.4 0.1 fusion.13
  12.5 2.8 %fusion = f32[16,4,1,256]{3,2,1,0:T(1,128)S(1)} fusion(bf16[16,16,4,8,256]{4,3,2,1,0:T(8,128)(2,1)} %bitcast.35, bf16[16,4,128,1]{2,1,0,3:T(4,128)(2,1)S(1)} %fusion.13), kind=kOutput, calls=%fused_computation | convolution fusion | flops 4194304 | bytes 4276224 | tf_op jit(solution)/shard_map/shj,sjhe->she/dot_general | solution.py:80
  15.3 4.2 %fusion.9 = f32[16,4,1,256]{3,2,1,0:T(1,128)S(1)} fusion(f32[16,4,128,256]{3,2,1,0:T(8,128)} %param.27, bf16[16,4,128,1]{2,1,0,3:T(4,128)(2,1)S(1)} %bitcast.37), kind=kOutput, calls=%fused_computation.28 | convolution fusion | flops 4194304 | bytes 8470528 | tf_op jit(solution)/shard_map/shd,shde->she/dot_general | solution.py:84
  19.5 0.0 copy-done.2
  19.5 0.0 copy-start.6
  19.5 0.0 copy-start.7
  19.6 0.0 copy-start.8
  19.6 0.4 convolution_convert_fusion
  20.0 0.1 multiply_exponential_fusion
  20.1 0.2 multiply_reduce_fusion.2
  20.3 0.1 multiply_convert_fusion.1
  20.4 0.5 multiply_reduce_fusion.1
  20.9 0.2 multiply_reduce_fusion
  21.2 0.7 %multiply_convert_fusion.nf_ref = bf16[16,1024]{1,0:T(8,128)(2,1)} fusion(f32[16,1024]{1,0:T(8,128)S(1)} %get-tuple-element.4.residual_ref, f32[1024]{0:T(1024)S(1)} %copy-done.6, f32[16]{0:T(128)S(1)} %add_rsqrt_fusion.1), kind=kLoop, calls=%fused_computation.13 | loop fusion | flops 49152 | bytes 102464 | tf_op jit(solution)/shard_map/convert_element_type | solution.py:492
  21.9 0.7 %copy.26.routes_ref = s32[16,6]{1,0:T(8,128)} copy(s32[16,6]{0,1:T(8,128)S(1)} %copy-done.7) | data formatting | bytes 768 | tf_op args[11]
  22.6 0.7 copy.27.scores_ref
  23.2 42.8 %layer.1 = bf16[16,1024]{1,0:T(8,128)(2,1)} custom-call(bf16[16,1024]{1,0:T(8,128)(2,1)} %multiply_convert_fusion.nf_ref, f32[16,1024]{1,0:T(8,128)} %copy-done.3, s32[16,6]{1,0:T(8,128)} %copy.26.routes_ref, f32[16,6]{1,0:T(8,128)} %copy.27.scores_ref, f32[1,1024]{1,0:T(1,128)} %bitcast.43, bf16[1,1024,256]{2,1,0:T(8,128)(2,1)} %eg_ref.1, ...), custom_call_target="tpu_custom_call" | custom-call | tf_op jit(solution)/shard_map/layer/pallas_call | solution.py:415
  66.0 0.6 copy.54
  66.6 1.4 %copy.56 = bf16[16,1024]{1,0:T(8,128)(2,1)} copy(bf16[16,1024]{1,0:T(8,128)(2,1)} %layer.1) | data formatting | bytes 65536
  (27 shorter events, 0.2 us)
Async XLA Ops:
  0.6 19.8 %copy-start = (bf16[1024,1024]{1,0:T(8,128)(2,1)S(1)}, bf16[1024,1024]{1,0:T(8,128)(2,1)}, u32[]{:S(2)}) copy-start(bf16[1024,1024]{1,0:T(8,128)(2,1)} %param.32) | copy-start | bytes 6291460
  9.9 2.2 %copy-start.9 = (s32[16]{0:T(128)S(1)}, s32[16]{0:T(128)}, u32[]{:S(2)}) copy-start(s32[16]{0:T(128)} %param.24) | copy-start | bytes 196
  15.3 4.2 %copy-start.1 = (bf16[1024,1024]{1,0:T(8,128)(2,1)S(1)}, bf16[1024,1024]{1,0:T(8,128)(2,1)}, u32[]{:S(2)}) copy-start(bf16[1024,1024]{1,0:T(8,128)(2,1)} %param.31) | copy-start | bytes 6291460
  15.3 4.2 %copy-start.2 = (bf16[16,1024]{1,0:T(8,128)(2,1)S(1)}, bf16[16,1024]{1,0:T(8,128)(2,1)}, u32[]{:S(2)}) copy-start(bf16[16,1024]{1,0:T(8,128)(2,1)} %param.23) | copy-start | bytes 98308
  15.3 4.2 %copy-start.5 = (f32[1024]{0:T(1024)S(1)}, f32[1024]{0:T(1024)}, u32[]{:S(2)}) copy-start(f32[1024]{0:T(1024)} %param.28) | copy-start | bytes 12292
  19.5 1.6 %copy-start.6 = (f32[1024]{0:T(1024)S(1)}, f32[1024]{0:T(1024)}, u32[]{:S(2)}) copy-start(f32[1024]{0:T(1024)} %param.33) | copy-start | bytes 12292
  19.5 2.3 %copy-start.7 = (s32[16,6]{0,1:T(8,128)S(1)}, s32[16,6]{0,1:T(8,128)}, u32[]{:S(2)}) copy-start(s32[16,6]{0,1:T(8,128)} %param.34) | copy-start | bytes 1156
  19.6 3.0 %copy-start.8 = (f32[16,6]{0,1:T(8,128)S(1)}, f32[16,6]{0,1:T(8,128)}, u32[]{:S(2)}) copy-start(f32[16,6]{0,1:T(8,128)} %param.35) | copy-start | bytes 1156
  20.0 46.0 %copy-start.4 = (bf16[16,1024]{1,0:T(8,128)(2,1)}, bf16[16,1024]{1,0:T(8,128)(2,1)S(1)}, u32[]{:S(2)}) copy-start(bf16[16,1024]{1,0:T(8,128)(2,1)S(1)} %convolution_convert_fusion) | copy-start | bytes 98308
  21.1 2.1 %copy-start.3 = (f32[16,1024]{1,0:T(8,128)}, f32[16,1024]{1,0:T(8,128)S(1)}, u32[]{:S(2)}) copy-start(f32[16,1024]{1,0:T(8,128)S(1)} %get-tuple-element.4.residual_ref) | copy-start | bytes 196612

commit v2 on v1

v2 whole, which is shorter than its diff:
```python
import math

import jax
import jax.numpy as jnp
from jax import lax
from jax.experimental import pallas as pl
from jax.experimental.pallas import tpu as pltpu
from jax.sharding import PartitionSpec as P

eps = 1e-06
route_scale = 2.5
rope_base = 10000.0
MESH = pl.DeviceIdType.MESH
F32 = jnp.float32
BF16 = jnp.bfloat16
N_DEV = 128
TOKENS = 16
WIDTH = 1024
TOP = 6
STEP = 53


def normed(values):
    return values * lax.rsqrt(jnp.mean(values * values, axis=-1, keepdims=True) + eps)


def dot(a, b):
    return jnp.dot(a, b, preferred_element_type=F32)


def dot_t(a, b):
    return lax.dot_general(a, b, (((1,), (1,)), ((), ())), preferred_element_type=F32)


def silu(v):
    return v / (1.0 + jnp.exp(-v))


def iota(shape, dim):
    return lax.broadcasted_iota(jnp.int32, shape, dim)


def one_hot(mask):
    return jnp.where(mask, 1.0, 0.0).astype(BF16)


def build_routing(routes_ref, scores_ref, place_ref, comb_ref):
    routes_t = routes_ref[...].astype(F32).astype(BF16)
    scores = scores_ref[...]
    weight = (scores / jnp.sum(scores, axis=0, keepdims=True) * route_scale).astype(BF16)
    small_eye = one_hot(iota((TOKENS, TOKENS), 0) == iota((TOKENS, TOKENS), 1))
    routes = dot_t(small_eye, routes_t)
    spread = one_hot((iota((TOKENS, 128), 1) & 15) == iota((TOKENS, 128), 0))
    spread_t = one_hot((iota((128, TOKENS), 0) & 15) == iota((128, TOKENS), 1))
    eye = one_hot(iota((128, 128), 0) == iota((128, 128), 1))
    lanes = dot(routes_t, spread)
    earlier = iota((TOKENS, 128), 0) < (iota((TOKENS, 128), 1) & 15)
    ranks = []
    for j in range(TOP):
        hits = jnp.zeros((TOKENS, 128), F32)
        for i in range(TOP):
            same = routes[:, i : i + 1] == lanes[j : j + 1, :]
            hits = hits + jnp.where(same & earlier, 1.0, 0.0)
        ranks.append(jnp.sum(hits, axis=0, keepdims=True))
    rank = jnp.concatenate(ranks, axis=0)
    chunk_lane = (iota((TOP, 128), 1) >> 4).astype(F32)
    code = lanes * 16.0 + chunk_lane * 2.0 + rank
    columns = dot_t(spread_t, routes_t)
    rank_columns = dot_t(eye, rank.astype(BF16))
    weight_columns = dot_t(spread_t, weight)
    code_t = columns * 16.0 + (iota((128, TOP), 0) >> 4).astype(F32) * 2.0 + rank_columns

    def place_rows(b, carry):
        at = pl.multiple_of(b * 128, 128)
        row = (iota((128, 128), 0) + at).astype(F32)
        found = row == code[0:1, :]
        for j in range(1, TOP):
            found = found | (row == code[j : j + 1, :])
        place_ref[pl.ds(at, 128), :] = one_hot(found)
        lane = (iota((128, 128), 1) + at).astype(F32)
        mixed = jnp.zeros((128, 128), F32)
        for j in range(TOP):
            mixed = jnp.where(lane == code_t[:, j : j + 1], weight_columns[:, j : j + 1], mixed)
        comb_ref[:, pl.ds(at, 128)] = mixed.astype(BF16)
        return carry

    lax.fori_loop(0, N_DEV * 16 // 128, place_rows, 0)


HEADS = 4
DK = 128
DV = 256
LOG_DECAY = [math.log1p(-(2.0 ** (-5 - h))) for h in range(HEADS)]


def rotation(lengths_ref):
    length = lengths_ref[...]
    both = jnp.concatenate([length >> 7, length & 127], axis=0).astype(F32).astype(BF16)
    eye = one_hot(iota((TOKENS, TOKENS), 0) == iota((TOKENS, TOKENS), 1))
    columns = dot_t(eye, both)
    filled = columns[:, 1:2]
    position = columns[:, 0:1] * 128.0 + filled
    place = (iota((TOKENS, DK), 1) & 63).astype(F32)
    angle = position * jnp.exp(place * (-math.log(rope_base) / 64.0))
    sine = jnp.sin(angle)
    signed = jnp.where(iota((TOKENS, DK), 1) < 64, -sine, sine)
    return jnp.cos(angle), signed, filled


def rotated(values, cosine, sine):
    parts = []
    for h in range(HEADS):
        v = values[:, h * DK : (h + 1) * DK]
        parts.append(v * cosine + pltpu.roll(v, 64, axis=1) * sine)
    return jnp.concatenate(parts, axis=1)


def layer_kernel(
    tokens_ref,
    lengths_ref,
    mixg_ref,
    ffng_ref,
    routes_ref,
    scores_ref,
    mix_ref,
    ck_ref,
    cv_ref,
    st_ref,
    wq_ref,
    wk_ref,
    wv_ref,
    wo_ref,
    eg_ref,
    eu_ref,
    ed_ref,
    sg_ref,
    su_ref,
    sd_ref,
    dg_ref,
    du_ref,
    dd_ref,
    out_ref,
    nk_ref,
    nv_ref,
    ck,
    cv,
    st,
    wq,
    wk,
    wv,
    wo,
    kept,
    place,
    comb,
    eg,
    eu,
    ed,
    sg,
    su,
    sd,
    dw,
    nf,
    snd,
    rcv,
    snd2,
    rcv2,
    acts,
    part,
    parts,
    rows,
    load_sem,
    ck_sem,
    cv_sem,
    st_sem,
    dense_load_sem,
    dw_send,
    dw_recv,
    fw_send,
    fw_recv,
    a2a_sem,
    ret_sem,
    act_sem,
    part_sem,
):
    me = lax.axis_index("ep")
    lane8 = lax.rem(me, 8)
    group = lax.div(me, 8)
    core = lax.rem(me, 2)
    base8 = group * 8
    sibling = me + 1 - 2 * core

    barrier = pltpu.get_barrier_semaphore()
    scope = jax.named_scope

    own_rows = pl.ds(pl.multiple_of(lane8 * 32, 32), 32)
    own_loads = [
        pltpu.make_async_copy(src, dw.at[i, own_rows], dense_load_sem.at[i])
        for i, src in enumerate((dg_ref, du_ref, dd_ref))
    ]
    wq_load, wk_load, wv_load, wo_load, *loads = [
        pltpu.make_async_copy(src, dst, load_sem.at[i])
        for i, (src, dst) in enumerate(
            (
                (wq_ref, wq),
                (wk_ref, wk),
                (wv_ref, wv),
                (wo_ref, wo),
                (sg_ref, sg),
                (su_ref, su),
                (sd_ref, sd),
                (eg_ref.at[0], eg),
                (eu_ref.at[0], eu),
                (ed_ref.at[0], ed),
            )
        )
    ]

    def pieces(source, target, sems, count):
        size = TOKENS // count
        return [
            pltpu.make_async_copy(
                source.at[pl.ds(i * size, size)], target.at[pl.ds(i * size, size)], sems.at[i]
            )
            for i in range(count)
        ]

    ck_loads = pieces(ck_ref, ck, ck_sem, 4)
    cv_loads = pieces(cv_ref, cv, cv_sem, 8)
    st_loads = pieces(st_ref, st, st_sem, 8)
    with scope("start"):
        for c in [*own_loads, wq_load, *ck_loads, *st_loads, wk_load, wv_load, *cv_loads, wo_load, *loads]:
            c.start()

        def greet(i, carry):
            peer = lax.rem(me + i, N_DEV)
            pl.semaphore_signal(barrier, inc=1, device_id=(peer,), device_id_type=MESH)
            return carry

        lax.fori_loop(1, N_DEV, greet, 0)

    with scope("routing"):
        build_routing(routes_ref, scores_ref, place, comb)

    def shard(slot):
        return dw.at[:, pl.ds(pl.multiple_of(slot * 32, 32), 32), :]

    with scope("greet_wait"):
        for c in own_loads:
            c.wait()
        pl.semaphore_wait(barrier, N_DEV - 1)
        weight_sends = []
        for i in range(4):
            peer = sibling if i == 0 else base8 + lax.rem(lane8 + 2 * i, 8)
            weight_sends.append(
                pltpu.make_async_remote_copy(
                    shard(lane8), shard(lane8), dw_send.at[i], dw_recv.at[i],
                    device_id=(peer,), device_id_type=MESH,
                )
            )
        for c in weight_sends:
            c.start()

    with scope("query"):
        widened = tokens_ref[...].astype(F32)
        normal_in = (normed(widened) * mixg_ref[...]).astype(BF16)
        cosine, sine, filled = rotation(lengths_ref)
        wq_load.wait()
        queries = (rotated(dot(normal_in, wq[...]), cosine, sine) * DK ** (-0.5)).astype(BF16)
        queries = queries.astype(F32)
        head_of_row = iota((8, HEADS * DK), 0)
        diagonal = head_of_row == (iota((8, HEADS * DK), 1) >> 7)
        spread_queries = [
            jnp.where(diagonal, queries[s : s + 1, :], 0.0).astype(BF16) for s in range(TOKENS)
        ]
        row8 = iota((8, 1), 0)
        decay = jnp.full((8, 1), LOG_DECAY[3], F32)
        for h in range(3):
            decay = jnp.where(row8 == h, LOG_DECAY[h], decay)
        places = iota((8, 128), 1).astype(F32)
    weights = []
    with scope("scores"):
        for i, c in enumerate(ck_loads):
            c.wait()
            for s in range(4 * i, 4 * i + 4):
                live = filled[s : s + 1, :] - places
                score = dot_t(spread_queries[s], ck[s])
                score = score * jnp.exp(jnp.maximum(live, 0.0) * decay)
                weights.append(jnp.where(live > 0.0, score, 0.0).astype(BF16))
    own_block = iota((8, HEADS * DV), 0) == (iota((8, HEADS * DV), 1) >> 8)
    carried = []
    with scope("state"):
        for i, c in enumerate(st_loads):
            c.wait()
            for s in range(2 * i, 2 * i + 2):
                state = st[s].reshape(HEADS * DK, DV).astype(BF16)
                taken = dot(spread_queries[s], state)
                carried.append(taken * jnp.exp((filled[s : s + 1, :] + 1.0) * decay))
    with scope("keys_values"):
        wk_load.wait()
        new_keys = rotated(dot(normal_in, wk[...]), cosine, sine).astype(BF16)
        nk_ref[...] = new_keys
        own = queries * new_keys.astype(F32)
        wv_load.wait()
        new_values = dot(normal_in, wv[...]).astype(BF16)
        nv_ref[...] = new_values
        new_values = new_values.astype(F32)
    with scope("values"):
        for i, c in enumerate(cv_loads):
            c.wait()
            for s in range(2 * i, 2 * i + 2):
                inside = dot(weights[s], cv[s])
                both = inside + jnp.concatenate([carried[s]] * HEADS, axis=1)
                kept[s : s + 1, :] = jnp.sum(jnp.where(own_block, both, 0.0), axis=0, keepdims=True)
    with scope("mix"):
        retained = kept[...]
        heads = []
        for h in range(HEADS):
            strength = jnp.sum(own[:, h * DK : (h + 1) * DK], axis=-1, keepdims=True)
            strength = strength.astype(BF16).astype(F32)
            cut = slice(h * DV, (h + 1) * DV)
            heads.append(normed(retained[:, cut] + strength * new_values[:, cut]).astype(BF16))
        wo_load.wait()
        mixer_out = dot(jnp.concatenate(heads, axis=1), wo[...])
        residual = widened + normed(mixer_out)
        nf_value = (normed(residual) * ffng_ref[...]).astype(BF16)

    with scope("dispatch"):
        nf[...] = nf_value
        stacked = jnp.concatenate([nf_value[:, k * 128 : (k + 1) * 128] for k in range(8)], axis=0)

        def pack(b, carry):
            at = pl.ds(pl.multiple_of(b * 256, 256), 256)
            snd[at, :] = dot(place[at, :], stacked).astype(BF16)
            return carry

        lax.fori_loop(0, 8, pack, 0)

        def tile(ref, index):
            return ref.at[pl.ds(pl.multiple_of(index * 16, 16), 16), :]

        def exchange(source, target, sems):
            def send(i, carry):
                peer = lax.rem(me + i * STEP, N_DEV)
                pltpu.make_async_remote_copy(
                    tile(source, peer), tile(target, me), sems.at[0], sems.at[1],
                    device_id=(peer,), device_id_type=MESH,
                ).start()
                return carry

            lax.fori_loop(1, N_DEV, send, 0)
            own = pl.ds(pl.multiple_of(me * 16, 16), 16)
            target[own, :] = source[own, :]

        def all_tiles(source, target, sems):
            whole = pl.ds(0, (N_DEV - 1) * 16)
            return pltpu.make_async_remote_copy(
                source.at[whole, :], target.at[whole, :], sems.at[0], sems.at[1],
                device_id=(sibling,), device_id_type=MESH,
            )

        exchange(snd, rcv, a2a_sem)

    with scope("acts"):
        act_rows = pl.ds(pl.multiple_of(group * 16, 16), 16)

        def send_acts(i, carry):
            peer = lax.rem(group + i, 16) * 8 + lane8
            pltpu.make_async_remote_copy(
                nf, acts.at[act_rows, :], act_sem.at[0], act_sem.at[1],
                device_id=(peer,), device_id_type=MESH,
            ).start()
            return carry

        lax.fori_loop(1, 16, send_acts, 0)
        acts[act_rows, :] = nf_value
    with scope("shared"):
        for c in loads[:3]:
            c.wait()
        hidden = (silu(dot(nf_value, sg[...])) * dot(nf_value, su[...])).astype(BF16)
        shared_out = dot(hidden, sd[...])

    with scope("swap_build"):
        rowi = iota((256, 256), 0)
        coli = iota((256, 256), 1)
        swap = one_hot(coli == ((rowi >> 1) & 15) * 16 + (rowi >> 5) * 2 + (rowi & 1))
        swap_t = one_hot(rowi == ((coli >> 1) & 15) * 16 + (coli >> 5) * 2 + (coli & 1))

        for c in loads[3:]:
            c.wait()
    with scope("wait_rows"):
        all_tiles(snd, rcv, a2a_sem).wait_recv()
    with scope("experts"):
        for b in range(8):
            moved = dot(swap, rcv[b * 256 : (b + 1) * 256, :]).astype(BF16)
            for k in range(8):
                rows[b * 32 : (b + 1) * 32, k * 128 : (k + 1) * 128] = moved[k * 32 : (k + 1) * 32, :]
        taken = rows[...]
        hidden = (silu(dot(taken, eg[...])) * dot(taken, eu[...])).astype(BF16)
        rows[...] = dot(hidden, ed[...]).astype(BF16)
        for b in range(8):
            piece = rows[b * 32 : (b + 1) * 32, :]
            column = jnp.concatenate([piece[:, k * 128 : (k + 1) * 128] for k in range(8)], axis=0)
            snd2[b * 256 : (b + 1) * 256, :] = dot(swap_t, column).astype(BF16)
    with scope("send_back"):
        exchange(snd2, rcv2, ret_sem)

    with scope("forward"):
        forwards = []
        for i in range(1, 4):
            slot = lax.rem(lane8 + 8 - 2 * i, 8)
            pltpu.make_async_remote_copy(
                shard(lane8), shard(slot), dw_send.at[i], dw_recv.at[i],
                device_id=(sibling,), device_id_type=MESH,
            ).wait_recv()
            c = pltpu.make_async_remote_copy(
                shard(slot), shard(slot), fw_send.at[i - 1], fw_recv.at[i - 1],
                device_id=(sibling,), device_id_type=MESH,
            )
            c.start()
            forwards.append(c)
    with scope("dense_wait"):
        for c in forwards:
            c.wait_recv()
        weight_sends[0].wait_recv()
        pltpu.make_async_remote_copy(
            acts.at[pl.ds(0, 240), :], acts.at[pl.ds(0, 240), :], act_sem.at[0], act_sem.at[1],
            device_id=(sibling,), device_id_type=MESH,
        ).wait_recv()
    with scope("dense"):
        every = acts[...]
        hidden = (silu(dot_t(every, dw[0])) * dot_t(every, dw[1])).astype(BF16)
        part[...] = dot(hidden, dw[2]).astype(BF16)

        def send_parts(i, carry):
            to = lax.rem(group + i, 16)
            pltpu.make_async_remote_copy(
                tile(part, to), tile(parts, group), part_sem.at[0], part_sem.at[1],
                device_id=(to * 8 + lane8,), device_id_type=MESH,
            ).start()
            return carry

        lax.fori_loop(1, 16, send_parts, 0)
        parts[act_rows, :] = part[act_rows, :]

    with scope("wait_back"):
        all_tiles(snd2, rcv2, ret_sem).wait_recv()
    with scope("combine"):
        mixed = dot(comb[...], rcv2[...])
        routed = jnp.concatenate([mixed[k * 16 : (k + 1) * 16, :] for k in range(8)], axis=1)
        gate = 1.0 / (1.0 + jnp.exp(-mix_ref[...]))

        all_parts = pltpu.make_async_remote_copy(
            part.at[pl.ds(0, 240), :], parts.at[pl.ds(0, 240), :], part_sem.at[0], part_sem.at[1],
            device_id=(sibling,), device_id_type=MESH,
        )
    with scope("wait_parts"):
        all_parts.wait_recv()
    with scope("final"):
        dense = parts[0:16, :].astype(F32)
        for g in range(1, 16):
            dense = dense + parts[g * 16 : (g + 1) * 16, :].astype(F32)
        combined = shared_out + routed + gate * dense
        out_ref[...] = (residual + normed(combined)).astype(BF16)

    with scope("drain"):
        for c in weight_sends:
            c.wait_send()
        for c in forwards:
            c.wait_send()
        all_tiles(snd, rcv, a2a_sem).wait_send()
        all_tiles(snd2, rcv2, ret_sem).wait_send()
        for sems in (act_sem,):
            pltpu.make_async_remote_copy(
                acts.at[pl.ds(0, 240), :], acts.at[pl.ds(0, 240), :], sems.at[0], sems.at[1],
                device_id=(sibling,), device_id_type=MESH,
            ).wait_send()
        all_parts.wait_send()


def run_layer(tokens, lengths, mix_gain, ffn_gain, routes, scores, mix, *large):
    vmem = pl.BlockSpec(memory_space=pltpu.VMEM)
    anywhere = pl.BlockSpec(memory_space=pl.ANY)
    dma = pltpu.SemaphoreType.DMA
    slots = (N_DEV * 16, 128)
    return pl.pallas_call(
        layer_kernel,
        name="layer",
        out_shape=(
            jax.ShapeDtypeStruct((TOKENS, WIDTH), BF16),
            jax.ShapeDtypeStruct((TOKENS, HEADS * DK), BF16),
            jax.ShapeDtypeStruct((TOKENS, HEADS * DV), BF16),
        ),
        in_specs=[vmem] * 7 + [anywhere] * 16,
        out_specs=(vmem, vmem, vmem),
        scratch_shapes=[
            pltpu.VMEM((TOKENS, 128, HEADS * DK), BF16),
            pltpu.VMEM((TOKENS, 128, HEADS * DV), BF16),
            pltpu.VMEM((TOKENS, HEADS, DK, DV), F32),
            pltpu.VMEM((WIDTH, HEADS * DK), BF16),
            pltpu.VMEM((WIDTH, HEADS * DK), BF16),
            pltpu.VMEM((WIDTH, HEADS * DV), BF16),
            pltpu.VMEM((HEADS * DV, WIDTH), BF16),
            pltpu.VMEM((TOKENS, HEADS * DV), F32),
            pltpu.VMEM(slots, BF16),
            pltpu.VMEM((128, N_DEV * 16), BF16),
            pltpu.VMEM((1024, 256), BF16),
            pltpu.VMEM((1024, 256), BF16),
            pltpu.VMEM((256, 1024), BF16),
            pltpu.VMEM((1024, 256), BF16),
            pltpu.VMEM((1024, 256), BF16),
            pltpu.VMEM((256, 1024), BF16),
            pltpu.VMEM((3, 256, 1024), BF16),
            pltpu.VMEM((TOKENS, WIDTH), BF16),
            pltpu.VMEM(slots, BF16),
            pltpu.VMEM(slots, BF16),
            pltpu.VMEM(slots, BF16),
            pltpu.VMEM(slots, BF16),
            pltpu.VMEM((256, 1024), BF16),
            pltpu.VMEM((256, 1024), BF16),
            pltpu.VMEM((256, 1024), BF16),
            pltpu.VMEM((256, 1024), BF16),
            dma((10,)),
            dma((4,)),
            dma((8,)),
            dma((8,)),
            dma((3,)),
            dma((4,)),
            dma((4,)),
            dma((3,)),
            dma((3,)),
            dma((2,)),
            dma((2,)),
            dma((2,)),
            dma((2,)),
        ],
        compiler_params=pltpu.CompilerParams(collective_id=0, has_side_effects=True),
    )(tokens, lengths, mix_gain, ffn_gain, routes, scores, mix, *large)


def per_device(
    tokens,
    lengths,
    cache_keys,
    cache_values,
    retention_state,
    mix_gain,
    query_weight,
    key_weight,
    value_weight,
    out_weight,
    ffn_gain,
    routes,
    route_scores,
    expert_gate,
    expert_up,
    expert_down,
    shared_gate,
    shared_up,
    shared_down,
    dense_gate,
    dense_up,
    dense_down,
    dense_mix,
):
    return run_layer(
        tokens,
        lengths[None, :],
        mix_gain[None, :],
        ffn_gain[None, :],
        routes.T,
        route_scores.T,
        dense_mix[None, :],
        cache_keys,
        cache_values,
        retention_state,
        query_weight,
        key_weight,
        value_weight,
        out_weight,
        expert_gate,
        expert_up,
        expert_down,
        shared_gate,
        shared_up,
        shared_down,
        dense_gate,
        dense_up,
        dense_down,
    )


def solution(mesh):
    in_specs = (
        P("ep", None),
        P("ep"),
        P("ep", None, None),
        P("ep", None, None),
        P("ep", None, None, None),
        P(),
        P(),
        P(),
        P(),
        P(),
        P(),
        P("ep", None),
        P("ep", None),
        P("ep", None, None),
        P("ep", None, None),
        P("ep", None, None),
        P(),
        P(),
        P(),
        P("ep", None),
        P("ep", None),
        P("ep", None),
        P(),
    )
    out_specs = (P("ep", None), P("ep", None), P("ep", None))
    return jax.shard_map(
        per_device, mesh=mesh, in_specs=in_specs, out_specs=out_specs, check_vma=False
    )
```

time: 68.4 us -> 54.1 us (0.79)
  matrix products: 13.3 us -> 0 us
  Pallas kernels: 42.8 us -> 49 us
  other arithmetic: 3.73 us -> 0 us
  local copies, waits for them, and re-layouts: 7.38 us -> 4.07 us
    dot_general x7 -> x0, matrix products: 13.3 us -> none  [the longest x1 4.19 us: retain(): jnp.einsum('shd,shde->she', queries.astype(jnp.float32), carry_state)]
    pallas_call x1, Pallas kernels: 42.8 us -> 49 us  [run_layer(): pl.pallas_call(layer_kernel, name='layer', out_shape=(jax.ShapeDtypeStruc...]
    reshape x3 -> x0, local copies, waits for them, and re-layouts: 3.94 us -> none  [the longest x1 3.91 us: retain(): cache_keys.reshape(seq_count, block_size, head_count, key_size)]
    convert_element_type x6 -> x0, other arithmetic: 1.61 us -> none  [the longest x1 0.69 us: per_device(): normal_ffn = (normed(residual) * ffn_gain).astype(jnp.bfloat16)]
    reduce_sum x4 -> x0, other arithmetic: 1.6 us -> none  [the longest x3 1.41 us: normed(): jnp.mean(values * values, axis=-1, keepdims=True) + eps]
    unnamed x25 -> x3, local copies, waits for them, and re-layouts: 3.4 us -> 4.07 us
where the time goes in v2:
time: 54.1 us; the launch traced here: 53.7 us
  Pallas kernels  49 us (91%)
  local copies, waits for them, and re-layouts  4.07 us (8%)
  between operations  0.65 us (1%)
    pallas_call x1, Pallas kernels, run_layer(): pl.pallas_call(layer_kernel, name='layer', out_shape=(jax.ShapeDtypeStruc...  49 us
    unnamed x3, local copies, waits for them, and re-layouts  4.07 us

profile of v2, /device:TPU:1, one launch (start us, length us, event | category | flops | bytes accessed | tf_op | source)
XLA Modules:
  0.0 53.7 jit_solution(10525390353742940833)
XLA Ops:
  0.6 49.0 %layer.1 = (bf16[16,1024]{1,0:T(8,128)(2,1)}, bf16[16,512]{1,0:T(8,128)(2,1)}, bf16[16,1024]{1,0:T(8,128)(2,1)}) custom-call(bf16[16,1024]{1,0:T(8,128)(2,1)} %tokens_ref.1, s32[1,16]{1,0:T(1,128)} %bitcast.11, f32[1,1024]{1,0:T(1,128)} %bitcast.6, f32[1,1024]{1,0:T(1,128)} %bitcast.7, s32[6,16]{1,0:T(8,128)} %bitcast.8, f32[6,16]{1,0:T(8,128)} %bitcast.9, ...), custom_call_target="tpu_custom_call" | custom-call | tf_op jit(solution)/shard_map/layer/pallas_call | solution.py:485
  49.6 1.4 %copy.29 = bf16[16,1024]{1,0:T(8,128)(2,1)} copy(bf16[16,1024]{1,0:T(8,128)(2,1)} %get-tuple-element.6) | data formatting | bytes 65536
  51.0 1.3 %copy.30 = bf16[16,512]{1,0:T(8,128)(2,1)} copy(bf16[16,512]{1,0:T(8,128)(2,1)} %get-tuple-element.7) | data formatting | bytes 32768
  52.3 1.4 %copy.31 = bf16[16,1024]{1,0:T(8,128)(2,1)} copy(bf16[16,1024]{1,0:T(8,128)(2,1)} %get-tuple-element.8) | data formatting | bytes 65536

commit v3 on v2

--- a/solution.py
+++ b/solution.py
@@ -17,7 +17,6 @@
 TOKENS = 16
 WIDTH = 1024
 TOP = 6
-STEP = 53
 
 
 def normed(values):
@@ -44,15 +43,15 @@
     return jnp.where(mask, 1.0, 0.0).astype(BF16)
 
 
-def build_routing(routes_ref, scores_ref, place_ref, comb_ref):
+def routing_codes(routes_ref, scores_ref):
     routes_t = routes_ref[...].astype(F32).astype(BF16)
     scores = scores_ref[...]
     weight = (scores / jnp.sum(scores, axis=0, keepdims=True) * route_scale).astype(BF16)
     small_eye = one_hot(iota((TOKENS, TOKENS), 0) == iota((TOKENS, TOKENS), 1))
-    routes = dot_t(small_eye, routes_t)
     spread = one_hot((iota((TOKENS, 128), 1) & 15) == iota((TOKENS, 128), 0))
     spread_t = one_hot((iota((128, TOKENS), 0) & 15) == iota((128, TOKENS), 1))
     eye = one_hot(iota((128, 128), 0) == iota((128, 128), 1))
+    routes = dot_t(small_eye, routes_t)
     lanes = dot(routes_t, spread)
     earlier = iota((TOKENS, 128), 0) < (iota((TOKENS, 128), 1) & 15)
     ranks = []
@@ -63,20 +62,26 @@
             hits = hits + jnp.where(same & earlier, 1.0, 0.0)
         ranks.append(jnp.sum(hits, axis=0, keepdims=True))
     rank = jnp.concatenate(ranks, axis=0)
-    chunk_lane = (iota((TOP, 128), 1) >> 4).astype(F32)
-    code = lanes * 16.0 + chunk_lane * 2.0 + rank
+    code = lanes * 2.0 + rank
     columns = dot_t(spread_t, routes_t)
     rank_columns = dot_t(eye, rank.astype(BF16))
     weight_columns = dot_t(spread_t, weight)
     code_t = columns * 16.0 + (iota((128, TOP), 0) >> 4).astype(F32) * 2.0 + rank_columns
-
-    def place_rows(b, carry):
+    return code, code_t, weight_columns
+
+
+def choose_rows(code, choose_ref):
+    row = iota((256, 128), 0).astype(F32)
+    found = row == code[0:1, :]
+    for j in range(1, TOP):
+        found = found | (row == code[j : j + 1, :])
+    found = found & (iota((256, 128), 1) < TOKENS)
+    choose_ref[...] = one_hot(found)
+
+
+def combine_rows(code_t, weight_columns, comb_ref):
+    def fill(b, carry):
         at = pl.multiple_of(b * 128, 128)
-        row = (iota((128, 128), 0) + at).astype(F32)
-        found = row == code[0:1, :]
-        for j in range(1, TOP):
-            found = found | (row == code[j : j + 1, :])
-        place_ref[pl.ds(at, 128), :] = one_hot(found)
         lane = (iota((128, 128), 1) + at).astype(F32)
         mixed = jnp.zeros((128, 128), F32)
         for j in range(TOP):
@@ -84,7 +89,7 @@
         comb_ref[:, pl.ds(at, 128)] = mixed.astype(BF16)
         return carry
 
-    lax.fori_loop(0, N_DEV * 16 // 128, place_rows, 0)
+    lax.fori_loop(0, N_DEV * 16 // 128, fill, 0)
 
 
 HEADS = 4
@@ -116,13 +121,13 @@
 
 
 def layer_kernel(
-    tokens_ref,
-    lengths_ref,
-    mixg_ref,
-    ffng_ref,
-    routes_ref,
-    scores_ref,
-    mix_ref,
+    tokens_hbm,
+    lengths_hbm,
+    mixg_hbm,
+    ffng_hbm,
+    routes_hbm,
+    scores_hbm,
+    mix_hbm,
     ck_ref,
     cv_ref,
     st_ref,
@@ -142,6 +147,13 @@
     out_ref,
     nk_ref,
     nv_ref,
+    tokens_ref,
+    lengths_ref,
+    mixg_ref,
+    ffng_ref,
+    routes_ref,
+    scores_ref,
+    mix_ref,
     ck,
     cv,
     st,
@@ -150,8 +162,9 @@
     wv,
     wo,
     kept,
-    place,
+    choose,
     comb,
+    swap_t,
     eg,
     eu,
     ed,
@@ -168,6 +181,7 @@
     part,
     parts,
     rows,
+    small_sem,
     load_sem,
     ck_sem,
     cv_sem,
@@ -227,38 +241,48 @@
     ck_loads = pieces(ck_ref, ck, ck_sem, 4)
     cv_loads = pieces(cv_ref, cv, cv_sem, 8)
     st_loads = pieces(st_ref, st, st_sem, 8)
+    small_loads = [
+        pltpu.make_async_copy(src, dst, small_sem.at[i])
+        for i, (src, dst) in enumerate(
+            (
+                (routes_hbm, routes_ref),
+                (scores_hbm, scores_ref),
+                (tokens_hbm, tokens_ref),
+                (lengths_hbm, lengths_ref),
+                (mixg_hbm, mixg_ref),
+                (ffng_hbm, ffng_ref),
+                (mix_hbm, mix_ref),
+            )
+        )
+    ]
     with scope("start"):
-        for c in [*own_loads, wq_load, *ck_loads, *st_loads, wk_load, wv_load, *cv_loads, wo_load, *loads]:
+        for c in [*small_loads, *own_loads, wq_load, *ck_loads]:
             c.start()
 
-        def greet(i, carry):
+        def greet(b, carry):
+            for i in range(16):
+                peer = lax.rem(me + b * 16 + i, N_DEV)
+                pl.semaphore_signal(barrier, inc=1, device_id=(peer,), device_id_type=MESH)
+            return carry
+
+        for i in range(1, 16):
             peer = lax.rem(me + i, N_DEV)
             pl.semaphore_signal(barrier, inc=1, device_id=(peer,), device_id_type=MESH)
-            return carry
-
-        lax.fori_loop(1, N_DEV, greet, 0)
+        lax.fori_loop(1, 8, greet, 0)
 
     with scope("routing"):
-        build_routing(routes_ref, scores_ref, place, comb)
+        rowi = iota((256, 256), 0)
+        coli = iota((256, 256), 1)
+        swap_t[...] = one_hot(rowi == ((coli >> 1) & 15) * 16 + (coli >> 5) * 2 + (coli & 1))
+        for c in small_loads:
+            c.wait()
+        for c in [wk_load, wv_load, *cv_loads[:4]]:
+            c.start()
+        code, code_t, weight_columns = routing_codes(routes_ref, scores_ref)
+        choose_rows(code, choose)
 
     def shard(slot):
         return dw.at[:, pl.ds(pl.multiple_of(slot * 32, 32), 32), :]
-
-    with scope("greet_wait"):
-        for c in own_loads:
-            c.wait()
-        pl.semaphore_wait(barrier, N_DEV - 1)
-        weight_sends = []
-        for i in range(4):
-            peer = sibling if i == 0 else base8 + lax.rem(lane8 + 2 * i, 8)
-            weight_sends.append(
-                pltpu.make_async_remote_copy(
-                    shard(lane8), shard(lane8), dw_send.at[i], dw_recv.at[i],
-                    device_id=(peer,), device_id_type=MESH,
-                )
-            )
-        for c in weight_sends:
-            c.start()
 
     with scope("query"):
         widened = tokens_ref[...].astype(F32)
@@ -279,6 +303,8 @@
         places = iota((8, 128), 1).astype(F32)
     weights = []
     with scope("scores"):
+        for c in [*cv_loads[4:], *st_loads[:4]]:
+            c.start()
         for i, c in enumerate(ck_loads):
             c.wait()
             for s in range(4 * i, 4 * i + 4):
@@ -286,16 +312,9 @@
                 score = dot_t(spread_queries[s], ck[s])
                 score = score * jnp.exp(jnp.maximum(live, 0.0) * decay)
                 weights.append(jnp.where(live > 0.0, score, 0.0).astype(BF16))
-    own_block = iota((8, HEADS * DV), 0) == (iota((8, HEADS * DV), 1) >> 8)
-    carried = []
-    with scope("state"):
-        for i, c in enumerate(st_loads):
-            c.wait()
-            for s in range(2 * i, 2 * i + 2):
-                state = st[s].reshape(HEADS * DK, DV).astype(BF16)
-                taken = dot(spread_queries[s], state)
-                carried.append(taken * jnp.exp((filled[s : s + 1, :] + 1.0) * decay))
     with scope("keys_values"):
+        for c in [*st_loads[4:], wo_load]:
+            c.start()
         wk_load.wait()
         new_keys = rotated(dot(normal_in, wk[...]), cosine, sine).astype(BF16)
         nk_ref[...] = new_keys
@@ -304,13 +323,23 @@
         new_values = dot(normal_in, wv[...]).astype(BF16)
         nv_ref[...] = new_values
         new_values = new_values.astype(F32)
+    own_block = iota((8, HEADS * DV), 0) == (iota((8, HEADS * DV), 1) >> 8)
     with scope("values"):
         for i, c in enumerate(cv_loads):
             c.wait()
             for s in range(2 * i, 2 * i + 2):
                 inside = dot(weights[s], cv[s])
-                both = inside + jnp.concatenate([carried[s]] * HEADS, axis=1)
-                kept[s : s + 1, :] = jnp.sum(jnp.where(own_block, both, 0.0), axis=0, keepdims=True)
+                kept[s : s + 1, :] = jnp.sum(jnp.where(own_block, inside, 0.0), axis=0, keepdims=True)
+    with scope("state"):
+        for c in loads:
+            c.start()
+        for i, c in enumerate(st_loads):
+            c.wait()
+            for s in range(2 * i, 2 * i + 2):
+                state = st[s].reshape(HEADS * DK, DV).astype(BF16)
+                carried = dot(spread_queries[s], state) * jnp.exp((filled[s : s + 1, :] + 1.0) * decay)
+                wide = jnp.concatenate([carried] * HEADS, axis=1)
+                kept[s : s + 1, :] += jnp.sum(jnp.where(own_block, wide, 0.0), axis=0, keepdims=True)
     with scope("mix"):
         retained = kept[...]
         heads = []
@@ -324,43 +353,63 @@
         residual = widened + normed(mixer_out)
         nf_value = (normed(residual) * ffng_ref[...]).astype(BF16)
 
-    with scope("dispatch"):
-        nf[...] = nf_value
-        stacked = jnp.concatenate([nf_value[:, k * 128 : (k + 1) * 128] for k in range(8)], axis=0)
-
-        def pack(b, carry):
-            at = pl.ds(pl.multiple_of(b * 256, 256), 256)
-            snd[at, :] = dot(place[at, :], stacked).astype(BF16)
-            return carry
-
-        lax.fori_loop(0, 8, pack, 0)
-
-        def tile(ref, index):
-            return ref.at[pl.ds(pl.multiple_of(index * 16, 16), 16), :]
-
-        def exchange(source, target, sems):
-            def send(i, carry):
-                peer = lax.rem(me + i * STEP, N_DEV)
+    def tile(ref, index):
+        return ref.at[pl.ds(pl.multiple_of(index * 16, 16), 16), :]
+
+    def exchange(source, target, sems):
+        def pack(b):
+            block = lax.rem(lax.div(me, 16) + b, 8)
+            piece = rows[pl.ds(pl.multiple_of(block * 32, 32), 32), :]
+            column = jnp.concatenate([piece[:, k * 128 : (k + 1) * 128] for k in range(8)], axis=0)
+            source[pl.ds(pl.multiple_of(block * 256, 256), 256), :] = dot(swap_t[...], column).astype(BF16)
+
+        def send(b, first):
+            block = lax.rem(lax.div(me, 16) + b, 8)
+            for i in range(first, 16):
+                peer = block * 16 + lax.rem(me + i, 16)
                 pltpu.make_async_remote_copy(
                     tile(source, peer), tile(target, me), sems.at[0], sems.at[1],
                     device_id=(peer,), device_id_type=MESH,
                 ).start()
-                return carry
-
-            lax.fori_loop(1, N_DEV, send, 0)
-            own = pl.ds(pl.multiple_of(me * 16, 16), 16)
-            target[own, :] = source[own, :]
-
-        def all_tiles(source, target, sems):
-            whole = pl.ds(0, (N_DEV - 1) * 16)
-            return pltpu.make_async_remote_copy(
-                source.at[whole, :], target.at[whole, :], sems.at[0], sems.at[1],
-                device_id=(sibling,), device_id_type=MESH,
+
+        def later(b, carry):
+            send(b, 0)
+            pack(lax.rem(b + 1, 8))
+            return carry
+
+        pack(1)
+        lax.fori_loop(1, 8, later, 0)
+        send(0, 1)
+        own = pl.ds(pl.multiple_of(me * 16, 16), 16)
+        target[own, :] = source[own, :]
+
+    def all_tiles(source, target, sems):
+        whole = pl.ds(0, (N_DEV - 1) * 16)
+        return pltpu.make_async_remote_copy(
+            source.at[whole, :], target.at[whole, :], sems.at[0], sems.at[1],
+            device_id=(sibling,), device_id_type=MESH,
+        )
+
+    with scope("greet_wait"):
+        for c in own_loads:
+            c.wait()
+        pl.semaphore_wait(barrier, N_DEV - 1)
+        weight_sends = []
+        for i in range(4):
+            peer = sibling if i == 0 else base8 + lax.rem(lane8 + 2 * i, 8)
+            weight_sends.append(
+                pltpu.make_async_remote_copy(
+                    shard(lane8), shard(lane8), dw_send.at[i], dw_recv.at[i],
+                    device_id=(peer,), device_id_type=MESH,
+                )
             )
 
+    with scope("dispatch"):
+        rows[...] = dot(choose[:, 0:TOKENS], nf_value).astype(BF16)
         exchange(snd, rcv, a2a_sem)
 
     with scope("acts"):
+        nf[...] = nf_value
         act_rows = pl.ds(pl.multiple_of(group * 16, 16), 16)
 
         def send_acts(i, carry):
@@ -373,6 +422,9 @@
 
         lax.fori_loop(1, 16, send_acts, 0)
         acts[act_rows, :] = nf_value
+    with scope("weights"):
+        for c in weight_sends:
+            c.start()
     with scope("shared"):
         for c in loads[:3]:
             c.wait()
@@ -380,11 +432,8 @@
         shared_out = dot(hidden, sd[...])
 
     with scope("swap_build"):
-        rowi = iota((256, 256), 0)
-        coli = iota((256, 256), 1)
         swap = one_hot(coli == ((rowi >> 1) & 15) * 16 + (rowi >> 5) * 2 + (rowi & 1))
-        swap_t = one_hot(rowi == ((coli >> 1) & 15) * 16 + (coli >> 5) * 2 + (coli & 1))
-
+        combine_rows(code_t, weight_columns, comb)
         for c in loads[3:]:
             c.wait()
     with scope("wait_rows"):
@@ -397,10 +446,6 @@
         taken = rows[...]
         hidden = (silu(dot(taken, eg[...])) * dot(taken, eu[...])).astype(BF16)
         rows[...] = dot(hidden, ed[...]).astype(BF16)
-        for b in range(8):
-            piece = rows[b * 32 : (b + 1) * 32, :]
-            column = jnp.concatenate([piece[:, k * 128 : (k + 1) * 128] for k in range(8)], axis=0)
-            snd2[b * 256 : (b + 1) * 256, :] = dot(swap_t, column).astype(BF16)
     with scope("send_back"):
         exchange(snd2, rcv2, ret_sem)
 
@@ -422,6 +467,7 @@
         for c in forwards:
             c.wait_recv()
         weight_sends[0].wait_recv()
+    with scope("acts_wait"):
         pltpu.make_async_remote_copy(
             acts.at[pl.ds(0, 240), :], acts.at[pl.ds(0, 240), :], act_sem.at[0], act_sem.at[1],
             device_id=(sibling,), device_id_type=MESH,
@@ -442,23 +488,22 @@
         lax.fori_loop(1, 16, send_parts, 0)
         parts[act_rows, :] = part[act_rows, :]
 
+    with scope("wait_parts"):
+        all_parts = pltpu.make_async_remote_copy(
+            part.at[pl.ds(0, 240), :], parts.at[pl.ds(0, 240), :], part_sem.at[0], part_sem.at[1],
+            device_id=(sibling,), device_id_type=MESH,
+        )
+        all_parts.wait_recv()
+        dense = parts[0:16, :].astype(F32)
+        for g in range(1, 16):
+            dense = dense + parts[g * 16 : (g + 1) * 16, :].astype(F32)
     with scope("wait_back"):
         all_tiles(snd2, rcv2, ret_sem).wait_recv()
     with scope("combine"):
         mixed = dot(comb[...], rcv2[...])
         routed = jnp.concatenate([mixed[k * 16 : (k + 1) * 16, :] for k in range(8)], axis=1)
         gate = 1.0 / (1.0 + jnp.exp(-mix_ref[...]))
-
-        all_parts = pltpu.make_async_remote_copy(
-            part.at[pl.ds(0, 240), :], parts.at[pl.ds(0, 240), :], part_sem.at[0], part_sem.at[1],
-            device_id=(sibling,), device_id_type=MESH,
-        )
-    with scope("wait_parts"):
-        all_parts.wait_recv()
     with scope("final"):
-        dense = parts[0:16, :].astype(F32)
-        for g in range(1, 16):
-            dense = dense + parts[g * 16 : (g + 1) * 16, :].astype(F32)
         combined = shared_out + routed + gate * dense
         out_ref[...] = (residual + normed(combined)).astype(BF16)
 
@@ -490,9 +535,16 @@
             jax.ShapeDtypeStruct((TOKENS, HEADS * DK), BF16),
             jax.ShapeDtypeStruct((TOKENS, HEADS * DV), BF16),
         ),
-        in_specs=[vmem] * 7 + [anywhere] * 16,
+        in_specs=[anywhere] * 23,
         out_specs=(vmem, vmem, vmem),
         scratch_shapes=[
+            pltpu.VMEM((TOKENS, WIDTH), BF16),
+            pltpu.VMEM((1, TOKENS), jnp.int32),
+            pltpu.VMEM((1, WIDTH), F32),
+            pltpu.VMEM((1, WIDTH), F32),
+            pltpu.VMEM((TOP, TOKENS), jnp.int32),
+            pltpu.VMEM((TOP, TOKENS), F32),
+            pltpu.VMEM((1, WIDTH), F32),
             pltpu.VMEM((TOKENS, 128, HEADS * DK), BF16),
             pltpu.VMEM((TOKENS, 128, HEADS * DV), BF16),
             pltpu.VMEM((TOKENS, HEADS, DK, DV), F32),
@@ -501,8 +553,9 @@
             pltpu.VMEM((WIDTH, HEADS * DV), BF16),
             pltpu.VMEM((HEADS * DV, WIDTH), BF16),
             pltpu.VMEM((TOKENS, HEADS * DV), F32),
-            pltpu.VMEM(slots, BF16),
+            pltpu.VMEM((256, 128), BF16),
             pltpu.VMEM((128, N_DEV * 16), BF16),
+            pltpu.VMEM((256, 256), BF16),
             pltpu.VMEM((1024, 256), BF16),
             pltpu.VMEM((1024, 256), BF16),
             pltpu.VMEM((256, 1024), BF16),
@@ -519,6 +572,7 @@
             pltpu.VMEM((256, 1024), BF16),
             pltpu.VMEM((256, 1024), BF16),
             pltpu.VMEM((256, 1024), BF16),
+            dma((7,)),
             dma((10,)),
             dma((4,)),
             dma((8,)),
@@ -535,6 +589,23 @@
         ],
         compiler_params=pltpu.CompilerParams(collective_id=0, has_side_effects=True),
     )(tokens, lengths, mix_gain, ffn_gain, routes, scores, mix, *large)
+
+
+def hand_over_kernel(a_ref, b_ref, c_ref, a_out, b_out, c_out):
+    a_out[...] = a_ref[...]
+    b_out[...] = b_ref[...]
+    c_out[...] = c_ref[...]
+
+
+def hand_over(*arrays):
+    vmem = pl.BlockSpec(memory_space=pltpu.VMEM)
+    return pl.pallas_call(
+        hand_over_kernel,
+        name="hand_over",
+        out_shape=tuple(jax.ShapeDtypeStruct(a.shape, a.dtype) for a in arrays),
+        in_specs=[vmem] * 3,
+        out_specs=(vmem,) * 3,
+    )(*arrays)
 
 
 def per_device(
@@ -562,7 +633,7 @@
     dense_down,
     dense_mix,
 ):
-    return run_layer(
+    layer_out, new_keys, new_values = run_layer(
         tokens,
         lengths[None, :],
         mix_gain[None, :],
@@ -587,6 +658,7 @@
         dense_up,
         dense_down,
     )
+    return hand_over(layer_out, new_keys, new_values)
 
 
 def solution(mesh):

time: 54.1 us -> 45.9 us (0.85)
  local copies, waits for them, and re-layouts: 4.07 us -> 0 us
  Pallas kernels: 49 us -> 45 us
    pallas_call x1, Pallas kernels: 49 us -> 43.6 us  [run_layer(): pl.pallas_call(layer_kernel, name='layer', out_shape=(jax.ShapeDtypeStruc...]
    unnamed x3 -> x0, local copies, waits for them, and re-layouts: 4.07 us -> none
    pallas_call x0 -> x1, Pallas kernels: none -> 1.43 us  [hand_over(): pl.pallas_call(hand_over_kernel, name='hand_over', out_shape=tuple((jax.S...]
where the time goes in v3:
time: 45.9 us; the launch traced here: 45.7 us
  Pallas kernels  45 us (98%)
  between operations  0.65 us (1%)
    pallas_call x1, Pallas kernels, run_layer(): pl.pallas_call(layer_kernel, name='layer', out_shape=(jax.ShapeDtypeStruc...  43.6 us
    pallas_call x1, Pallas kernels, hand_over(): pl.pallas_call(hand_over_kernel, name='hand_over', out_shape=tuple((jax.S...  1.43 us

profile of v3, /device:TPU:1, one launch (start us, length us, event | category | flops | bytes accessed | tf_op | source)
XLA Modules:
  0.0 45.7 jit_solution(14750910121899583812)
XLA Ops:
  0.6 43.6 %layer.1 = (bf16[16,1024]{1,0:T(8,128)(2,1)}, bf16[16,512]{1,0:T(8,128)(2,1)}, bf16[16,1024]{1,0:T(8,128)(2,1)}) custom-call(bf16[16,1024]{1,0:T(8,128)(2,1)} %tokens_hbm.1, s32[1,16]{1,0:T(1,128)} %bitcast.11, f32[1,1024]{1,0:T(1,128)} %bitcast.6, f32[1,1024]{1,0:T(1,128)} %bitcast.7, s32[6,16]{1,0:T(8,128)} %bitcast.8, f32[6,16]{1,0:T(8,128)} %bitcast.9, ...), custom_call_target="tpu_custom_call" | custom-call | tf_op jit(solution)/shard_map/layer/pallas_call | solution.py:530
  44.3 1.4 %hand_over.1 = (bf16[16,1024]{1,0:T(8,128)(2,1)}, bf16[16,512]{1,0:T(8,128)(2,1)}, bf16[16,1024]{1,0:T(8,128)(2,1)}) custom-call(bf16[16,1024]{1,0:T(8,128)(2,1)} %get-tuple-element.6.a_ref, bf16[16,512]{1,0:T(8,128)(2,1)} %get-tuple-element.7.b_ref, bf16[16,1024]{1,0:T(8,128)(2,1)} %get-tuple-element.8.c_ref), custom_call_target="tpu_custom_call" | custom-call | tf_op jit(solution)/shard_map/hand_over/pallas_call | solution.py:602

commit v4 on v3

--- a/solution.py
+++ b/solution.py
@@ -43,14 +43,10 @@
     return jnp.where(mask, 1.0, 0.0).astype(BF16)
 
 
-def routing_codes(routes_ref, scores_ref):
+def routing_codes(routes_ref):
     routes_t = routes_ref[...].astype(F32).astype(BF16)
-    scores = scores_ref[...]
-    weight = (scores / jnp.sum(scores, axis=0, keepdims=True) * route_scale).astype(BF16)
     small_eye = one_hot(iota((TOKENS, TOKENS), 0) == iota((TOKENS, TOKENS), 1))
     spread = one_hot((iota((TOKENS, 128), 1) & 15) == iota((TOKENS, 128), 0))
-    spread_t = one_hot((iota((128, TOKENS), 0) & 15) == iota((128, TOKENS), 1))
-    eye = one_hot(iota((128, 128), 0) == iota((128, 128), 1))
     routes = dot_t(small_eye, routes_t)
     lanes = dot(routes_t, spread)
     earlier = iota((TOKENS, 128), 0) < (iota((TOKENS, 128), 1) & 15)
@@ -62,12 +58,20 @@
             hits = hits + jnp.where(same & earlier, 1.0, 0.0)
         ranks.append(jnp.sum(hits, axis=0, keepdims=True))
     rank = jnp.concatenate(ranks, axis=0)
-    code = lanes * 2.0 + rank
+    return lanes * 2.0 + rank, rank
+
+
+def column_codes(routes_ref, scores_ref, rank):
+    routes_t = routes_ref[...].astype(F32).astype(BF16)
+    scores = scores_ref[...]
+    weight = (scores / jnp.sum(scores, axis=0, keepdims=True) * route_scale).astype(BF16)
+    spread_t = one_hot((iota((128, TOKENS), 0) & 15) == iota((128, TOKENS), 1))
+    eye = one_hot(iota((128, 128), 0) == iota((128, 128), 1))
     columns = dot_t(spread_t, routes_t)
     rank_columns = dot_t(eye, rank.astype(BF16))
     weight_columns = dot_t(spread_t, weight)
     code_t = columns * 16.0 + (iota((128, TOP), 0) >> 4).astype(F32) * 2.0 + rank_columns
-    return code, code_t, weight_columns
+    return code_t, weight_columns
 
 
 def choose_rows(code, choose_ref):
@@ -278,7 +282,7 @@
             c.wait()
         for c in [wk_load, wv_load, *cv_loads[:4]]:
             c.start()
-        code, code_t, weight_columns = routing_codes(routes_ref, scores_ref)
+        code, rank = routing_codes(routes_ref)
         choose_rows(code, choose)
 
     def shard(slot):
@@ -330,6 +334,23 @@
             for s in range(2 * i, 2 * i + 2):
                 inside = dot(weights[s], cv[s])
                 kept[s : s + 1, :] = jnp.sum(jnp.where(own_block, inside, 0.0), axis=0, keepdims=True)
+    with scope("greet_wait"):
+        for c in own_loads:
+            c.wait()
+        pl.semaphore_wait(barrier, N_DEV - 1)
+        weight_sends = []
+        for which, first in ((slice(0, 1), 0), (slice(1, 3), 4)):
+            for i in range(4):
+                peer = sibling if i == 0 else base8 + lax.rem(lane8 + 2 * i, 8)
+                mine = dw.at[which, pl.ds(pl.multiple_of(lane8 * 32, 32), 32), :]
+                weight_sends.append(
+                    pltpu.make_async_remote_copy(
+                        mine, mine, dw_send.at[first + i], dw_recv.at[first + i],
+                        device_id=(peer,), device_id_type=MESH,
+                    )
+                )
+        for c in weight_sends[:4]:
+            c.start()
     with scope("state"):
         for c in loads:
             c.start()
@@ -390,20 +411,6 @@
             device_id=(sibling,), device_id_type=MESH,
         )
 
-    with scope("greet_wait"):
-        for c in own_loads:
-            c.wait()
-        pl.semaphore_wait(barrier, N_DEV - 1)
-        weight_sends = []
-        for i in range(4):
-            peer = sibling if i == 0 else base8 + lax.rem(lane8 + 2 * i, 8)
-            weight_sends.append(
-                pltpu.make_async_remote_copy(
-                    shard(lane8), shard(lane8), dw_send.at[i], dw_recv.at[i],
-                    device_id=(peer,), device_id_type=MESH,
-                )
-            )
-
     with scope("dispatch"):
         rows[...] = dot(choose[:, 0:TOKENS], nf_value).astype(BF16)
         exchange(snd, rcv, a2a_sem)
@@ -423,7 +430,7 @@
         lax.fori_loop(1, 16, send_acts, 0)
         acts[act_rows, :] = nf_value
     with scope("weights"):
-        for c in weight_sends:
+        for c in weight_sends[4:]:
             c.start()
     with scope("shared"):
         for c in loads[:3]:
@@ -433,9 +440,25 @@
 
     with scope("swap_build"):
         swap = one_hot(coli == ((rowi >> 1) & 15) * 16 + (rowi >> 5) * 2 + (rowi & 1))
+        code_t, weight_columns = column_codes(routes_ref, scores_ref, rank)
         combine_rows(code_t, weight_columns, comb)
         for c in loads[3:]:
             c.wait()
+    def forward(which, first):
+        for i in range(1, 4):
+            slot = lax.rem(lane8 + 8 - 2 * i, 8)
+            weight_sends[first + i].wait_recv()
+            there = dw.at[which, pl.ds(pl.multiple_of(slot * 32, 32), 32), :]
+            c = pltpu.make_async_remote_copy(
+                there, there, fw_send.at[first + i], fw_recv.at[first + i],
+                device_id=(sibling,), device_id_type=MESH,
+            )
+            c.start()
+            forwards.append(c)
+
+    forwards = []
+    with scope("forward_gate"):
+        forward(slice(0, 1), 0)
     with scope("wait_rows"):
         all_tiles(snd, rcv, a2a_sem).wait_recv()
     with scope("experts"):
@@ -450,23 +473,12 @@
         exchange(snd2, rcv2, ret_sem)
 
     with scope("forward"):
-        forwards = []
-        for i in range(1, 4):
-            slot = lax.rem(lane8 + 8 - 2 * i, 8)
-            pltpu.make_async_remote_copy(
-                shard(lane8), shard(slot), dw_send.at[i], dw_recv.at[i],
-                device_id=(sibling,), device_id_type=MESH,
-            ).wait_recv()
-            c = pltpu.make_async_remote_copy(
-                shard(slot), shard(slot), fw_send.at[i - 1], fw_recv.at[i - 1],
-                device_id=(sibling,), device_id_type=MESH,
-            )
-            c.start()
-            forwards.append(c)
+        forward(slice(1, 3), 4)
     with scope("dense_wait"):
         for c in forwards:
             c.wait_recv()
         weight_sends[0].wait_recv()
+        weight_sends[4].wait_recv()
     with scope("acts_wait"):
         pltpu.make_async_remote_copy(
             acts.at[pl.ds(0, 240), :], acts.at[pl.ds(0, 240), :], act_sem.at[0], act_sem.at[1],
@@ -488,6 +500,12 @@
         lax.fori_loop(1, 16, send_parts, 0)
         parts[act_rows, :] = part[act_rows, :]
 
+    with scope("wait_back"):
+        all_tiles(snd2, rcv2, ret_sem).wait_recv()
+    with scope("combine"):
+        mixed = dot(comb[...], rcv2[...])
+        routed = jnp.concatenate([mixed[k * 16 : (k + 1) * 16, :] for k in range(8)], axis=1)
+        gate = 1.0 / (1.0 + jnp.exp(-mix_ref[...]))
     with scope("wait_parts"):
         all_parts = pltpu.make_async_remote_copy(
             part.at[pl.ds(0, 240), :], parts.at[pl.ds(0, 240), :], part_sem.at[0], part_sem.at[1],
@@ -497,12 +515,6 @@
         dense = parts[0:16, :].astype(F32)
         for g in range(1, 16):
             dense = dense + parts[g * 16 : (g + 1) * 16, :].astype(F32)
-    with scope("wait_back"):
-        all_tiles(snd2, rcv2, ret_sem).wait_recv()
-    with scope("combine"):
-        mixed = dot(comb[...], rcv2[...])
-        routed = jnp.concatenate([mixed[k * 16 : (k + 1) * 16, :] for k in range(8)], axis=1)
-        gate = 1.0 / (1.0 + jnp.exp(-mix_ref[...]))
     with scope("final"):
         combined = shared_out + routed + gate * dense
         out_ref[...] = (residual + normed(combined)).astype(BF16)
@@ -531,9 +543,9 @@
         layer_kernel,
         name="layer",
         out_shape=(
-            jax.ShapeDtypeStruct((TOKENS, WIDTH), BF16),
-            jax.ShapeDtypeStruct((TOKENS, HEADS * DK), BF16),
-            jax.ShapeDtypeStruct((TOKENS, HEADS * DV), BF16),
+            pltpu.VMEM((TOKENS, WIDTH), BF16),
+            pltpu.VMEM((TOKENS, HEADS * DK), BF16),
+            pltpu.VMEM((TOKENS, HEADS * DV), BF16),
         ),
         in_specs=[anywhere] * 23,
         out_specs=(vmem, vmem, vmem),
@@ -578,10 +590,10 @@
             dma((8,)),
             dma((8,)),
             dma((3,)),
-            dma((4,)),
-            dma((4,)),
-            dma((3,)),
-            dma((3,)),
+            dma((8,)),
+            dma((8,)),
+            dma((8,)),
+            dma((8,)),
             dma((2,)),
             dma((2,)),
             dma((2,)),
@@ -605,7 +617,7 @@
         out_shape=tuple(jax.ShapeDtypeStruct(a.shape, a.dtype) for a in arrays),
         in_specs=[vmem] * 3,
         out_specs=(vmem,) * 3,
-    )(*arrays)
+    )(*(pltpu.with_memory_space_constraint(a, pltpu.VMEM) for a in arrays))
 
 
 def per_device(

time: 45.9 us -> 42.4 us (0.924)
  Pallas kernels: 45 us -> 41.6 us
    pallas_call x1, Pallas kernels: 43.6 us -> 41 us  [run_layer(): pl.pallas_call(layer_kernel, name='layer', out_shape=(pltpu.VMEM((TOKENS,...]
    pallas_call x1, Pallas kernels: 1.43 us -> 0.64 us  [hand_over(): pl.pallas_call(hand_over_kernel, name='hand_over', out_shape=tuple((jax.S...]
where the time goes in v4:
time: 42.4 us; the launch traced here: 42.3 us
  Pallas kernels  41.6 us (98%)
  between operations  0.65 us (2%)
    pallas_call x1, Pallas kernels, run_layer(): pl.pallas_call(layer_kernel, name='layer', out_shape=(pltpu.VMEM((TOKENS,...  41 us

profile of v4, /device:TPU:1, one launch (start us, length us, event | category | flops | bytes accessed | tf_op | source)
XLA Modules:
  0.0 42.3 jit_solution(4951160697829405135)
XLA Ops:
  0.6 41.0 %layer.1 = (bf16[16,1024]{1,0:T(8,128)(2,1)S(1)}, bf16[16,512]{1,0:T(8,128)(2,1)S(1)}, bf16[16,1024]{1,0:T(8,128)(2,1)S(1)}) custom-call(bf16[16,1024]{1,0:T(8,128)(2,1)} %tokens_hbm.1, s32[1,16]{1,0:T(1,128)} %bitcast.11, f32[1,1024]{1,0:T(1,128)} %bitcast.6, f32[1,1024]{1,0:T(1,128)} %bitcast.7, s32[6,16]{1,0:T(8,128)} %bitcast.8, f32[6,16]{1,0:T(8,128)} %bitcast.9, ...), custom_call_target="tpu_custom_call" | custom-call | tf_op jit(solution)/shard_map/layer/pallas_call | solution.py:542
  41.6 0.6 %hand_over.1 = (bf16[16,1024]{1,0:T(8,128)(2,1)}, bf16[16,512]{1,0:T(8,128)(2,1)}, bf16[16,1024]{1,0:T(8,128)(2,1)}) custom-call(bf16[16,1024]{1,0:T(8,128)(2,1)S(1)} %get-tuple-element.6.a_ref, bf16[16,512]{1,0:T(8,128)(2,1)S(1)} %get-tuple-element.7.b_ref, bf16[16,1024]{1,0:T(8,128)(2,1)S(1)} %get-tuple-element.8.c_ref), custom_call_target="tpu_custom_call" | custom-call | tf_op jit(solution)/shard_map/hand_over/pallas_call | solution.py:614

commit v5 on v4

--- a/solution.py
+++ b/solution.py
@@ -384,30 +384,34 @@
             column = jnp.concatenate([piece[:, k * 128 : (k + 1) * 128] for k in range(8)], axis=0)
             source[pl.ds(pl.multiple_of(block * 256, 256), 256), :] = dot(swap_t[...], column).astype(BF16)
 
-        def send(b, first):
+        def send(b, first, late):
             block = lax.rem(lax.div(me, 16) + b, 8)
             for i in range(first, 16):
                 peer = block * 16 + lax.rem(me + i, 16)
                 pltpu.make_async_remote_copy(
-                    tile(source, peer), tile(target, me), sems.at[0], sems.at[1],
+                    tile(source, peer), tile(target, me), sems.at[0], sems.at[late],
                     device_id=(peer,), device_id_type=MESH,
                 ).start()
 
-        def later(b, carry):
-            send(b, 0)
-            pack(lax.rem(b + 1, 8))
-            return carry
+        def step(late):
+            def body(b, carry):
+                send(b, 0, late)
+                pack(lax.rem(b + 1, 8))
+                return carry
+
+            return body
 
         pack(1)
-        lax.fori_loop(1, 8, later, 0)
-        send(0, 1)
+        lax.fori_loop(1, 4, step(1), 0)
+        lax.fori_loop(4, 8, step(2), 0)
+        send(0, 1, 1)
         own = pl.ds(pl.multiple_of(me * 16, 16), 16)
         target[own, :] = source[own, :]
 
-    def all_tiles(source, target, sems):
-        whole = pl.ds(0, (N_DEV - 1) * 16)
+    def tiles(source, target, sems, count, late):
+        whole = pl.ds(0, count * 16)
         return pltpu.make_async_remote_copy(
-            source.at[whole, :], target.at[whole, :], sems.at[0], sems.at[1],
+            source.at[whole, :], target.at[whole, :], sems.at[0], sems.at[late],
             device_id=(sibling,), device_id_type=MESH,
         )
 
@@ -459,13 +463,22 @@
     forwards = []
     with scope("forward_gate"):
         forward(slice(0, 1), 0)
+    def unpack(b):
+        block = lax.rem(lax.div(me, 16) + 8 - b, 8)
+        moved = dot(swap, rcv[pl.ds(pl.multiple_of(block * 256, 256), 256), :]).astype(BF16)
+        at = pl.ds(pl.multiple_of(block * 32, 32), 32)
+        for k in range(8):
+            rows[at, k * 128 : (k + 1) * 128] = moved[k * 32 : (k + 1) * 32, :]
+
     with scope("wait_rows"):
-        all_tiles(snd, rcv, a2a_sem).wait_recv()
+        tiles(snd, rcv, a2a_sem, 63, 1).wait_recv()
+        for b in range(4):
+            unpack(b)
+    with scope("wait_rows_far"):
+        tiles(snd, rcv, a2a_sem, 64, 2).wait_recv()
     with scope("experts"):
-        for b in range(8):
-            moved = dot(swap, rcv[b * 256 : (b + 1) * 256, :]).astype(BF16)
-            for k in range(8):
-                rows[b * 32 : (b + 1) * 32, k * 128 : (k + 1) * 128] = moved[k * 32 : (k + 1) * 32, :]
+        for b in range(4, 8):
+            unpack(b)
         taken = rows[...]
         hidden = (silu(dot(taken, eg[...])) * dot(taken, eu[...])).astype(BF16)
         rows[...] = dot(hidden, ed[...]).astype(BF16)
@@ -501,7 +514,8 @@
         parts[act_rows, :] = part[act_rows, :]
 
     with scope("wait_back"):
-        all_tiles(snd2, rcv2, ret_sem).wait_recv()
+        tiles(snd2, rcv2, ret_sem, 63, 1).wait_recv()
+        tiles(snd2, rcv2, ret_sem, 64, 2).wait_recv()
     with scope("combine"):
         mixed = dot(comb[...], rcv2[...])
         routed = jnp.concatenate([mixed[k * 16 : (k + 1) * 16, :] for k in range(8)], axis=1)
@@ -524,8 +538,8 @@
             c.wait_send()
         for c in forwards:
             c.wait_send()
-        all_tiles(snd, rcv, a2a_sem).wait_send()
-        all_tiles(snd2, rcv2, ret_sem).wait_send()
+        tiles(snd, rcv, a2a_sem, N_DEV - 1, 1).wait_send()
+        tiles(snd2, rcv2, ret_sem, N_DEV - 1, 1).wait_send()
         for sems in (act_sem,):
             pltpu.make_async_remote_copy(
                 acts.at[pl.ds(0, 240), :], acts.at[pl.ds(0, 240), :], sems.at[0], sems.at[1],
@@ -594,8 +608,8 @@
             dma((8,)),
             dma((8,)),
             dma((8,)),
-            dma((2,)),
-            dma((2,)),
+            dma((3,)),
+            dma((3,)),
             dma((2,)),
             dma((2,)),
         ],
@@ -603,10 +617,15 @@
     )(tokens, lengths, mix_gain, ffn_gain, routes, scores, mix, *large)
 
 
-def hand_over_kernel(a_ref, b_ref, c_ref, a_out, b_out, c_out):
-    a_out[...] = a_ref[...]
-    b_out[...] = b_ref[...]
-    c_out[...] = c_ref[...]
+def hand_over_kernel(a_ref, b_ref, c_ref, a_out, b_out, c_out, sems):
+    copies = [
+        pltpu.make_async_copy(source, target, sems.at[i])
+        for i, (source, target) in enumerate(((a_ref, a_out), (b_ref, b_out), (c_ref, c_out)))
+    ]
+    for c in copies:
+        c.start()
+    for c in copies:
+        c.wait()
 
 
 def hand_over(*arrays):
@@ -616,7 +635,8 @@
         name="hand_over",
         out_shape=tuple(jax.ShapeDtypeStruct(a.shape, a.dtype) for a in arrays),
         in_specs=[vmem] * 3,
-        out_specs=(vmem,) * 3,
+        out_specs=(pl.BlockSpec(memory_space=pltpu.HBM),) * 3,
+        scratch_shapes=[pltpu.SemaphoreType.DMA((3,))],
     )(*(pltpu.with_memory_space_constraint(a, pltpu.VMEM) for a in arrays))
 
 

time: 42.4 us -> 42.4 us (level)
  no operation moved by 1% of the time
where the time goes in v5:
time: 42.4 us; the launch traced here: 42.3 us
  Pallas kernels  41.6 us (98%)
  between operations  0.65 us (2%)
    pallas_call x1, Pallas kernels, run_layer(): pl.pallas_call(layer_kernel, name='layer', out_shape=(pltpu.VMEM((TOKENS,...  41 us

profile of v5, /device:TPU:1, one launch (start us, length us, event | category | flops | bytes accessed | tf_op | source)
XLA Modules:
  0.0 42.3 jit_solution(6619965044015653273)
XLA Ops:
  0.6 41.0 %layer.1 = (bf16[16,1024]{1,0:T(8,128)(2,1)S(1)}, bf16[16,512]{1,0:T(8,128)(2,1)S(1)}, bf16[16,1024]{1,0:T(8,128)(2,1)S(1)}) custom-call(bf16[16,1024]{1,0:T(8,128)(2,1)} %tokens_hbm.1, s32[1,16]{1,0:T(1,128)} %bitcast.11, f32[1,1024]{1,0:T(1,128)} %bitcast.6, f32[1,1024]{1,0:T(1,128)} %bitcast.7, s32[6,16]{1,0:T(8,128)} %bitcast.8, f32[6,16]{1,0:T(8,128)} %bitcast.9, ...), custom_call_target="tpu_custom_call" | custom-call | tf_op jit(solution)/shard_map/layer/pallas_call | solution.py:556
  41.6 0.7 %hand_over.1 = (bf16[16,1024]{1,0:T(8,128)(2,1)}, bf16[16,512]{1,0:T(8,128)(2,1)}, bf16[16,1024]{1,0:T(8,128)(2,1)}) custom-call(bf16[16,1024]{1,0:T(8,128)(2,1)S(1)} %get-tuple-element.6.a_ref, bf16[16,512]{1,0:T(8,128)(2,1)S(1)} %get-tuple-element.7.b_ref, bf16[16,1024]{1,0:T(8,128)(2,1)S(1)} %get-tuple-element.8.c_ref), custom_call_target="tpu_custom_call" | custom-call | tf_op jit(solution)/shard_map/hand_over/pallas_call | solution.py:633
